TPU v7x, 128 devices: a whole 4x4x4 slice. The times are simulated.
128 devices in a mesh: fs: 16 (over z, y), tp: 8 (over x, core).
Axes of the slice: x: 4, y: 4, z: 4, core: 2. Of those that a mesh axis runs over, the one named last changes fastest.
Arguments:
- normed_input: bfloat16 [24576, 2048], P(('fs', 'tp')), may hold values from -6 to 6
- pre_act: bfloat16 [24576, 8192], P('fs', 'tp'), may hold values from -6 to 6
- out_grad: bfloat16 [24576, 2048], P(('fs', 'tp')), may hold values from -24 to 24
- up_weight: bfloat16 [2048, 8192], P('fs', 'tp'), may hold values from -0.125 to 0.125
- down_weight: bfloat16 [8192, 2048], P('tp', 'fs'), may hold values from -0.0625 to 0.0625
Outputs:
- input_grad: bfloat16 [24576, 2048], P(('fs', 'tp'))
- up_grad: float32 [2048, 8192], P('fs', 'tp')
- down_grad: float32 [8192, 2048], P('tp', 'fs')
All inputs are finite; a program needn't handle non-finite values.
Results may differ from a plain program's by a relative error of at most 0.014.
Values may be sent and summed in bfloat16 or wider, within the bound.
A program may use at most 128 MiB of HBM per device.

v0:
```python
import jax
import jax.numpy as jnp
from jax import lax
from jax.sharding import PartitionSpec as P


def sent_together(arrays, axis, dim, along):
    ends, at = ([], 0)
    for a in arrays[:-1]:
        at += a.shape[along]
        ends.append(at)
    both = jnp.concatenate(arrays, axis=along)
    return tuple(jnp.split(lax.all_gather(both, axis, axis=dim, tiled=True), ends, axis=along))


def cut_along(x, dim, count):
    before, after = (x.shape[:dim], x.shape[dim + 1 :])
    return jnp.moveaxis(x.reshape(*before, count, -1, *after), dim, 0)


def sum_at_owner(x, axis, dim):
    tiles = cut_along(x, dim, lax.axis_size(axis))
    arrived = lax.all_to_all(tiles, axis, split_axis=0, concat_axis=0, tiled=True)
    return arrived.astype(jnp.float32).sum(axis=0)


def local(normed_input, pre_act, out_grad, up_weight, down_weight):
    rows_all, grad_rows = sent_together((normed_input, out_grad), "tp", 0, 1)
    active = jnp.maximum(pre_act.astype(jnp.float32), 0.0)
    hidden = (active * active).astype(jnp.bfloat16)
    width = pre_act.shape[1]
    columns = grad_rows
    hidden_grad = jnp.dot(
        columns,
        lax.all_gather(down_weight, "fs", axis=1, tiled=True).T,
        preferred_element_type=jnp.float32,
    )
    pre_grad = (2.0 * active * hidden_grad).astype(jnp.bfloat16)
    partial_value = jnp.dot(
        pre_grad,
        lax.all_gather(up_weight, "fs", axis=0, tiled=True).T,
        preferred_element_type=jnp.float32,
    )
    rounded = lax.optimization_barrier(partial_value.astype(jnp.bfloat16))
    summed = sum_at_owner(rounded.astype(jnp.float32).astype(jnp.bfloat16), "tp", 0)
    input_grad = summed.astype(jnp.bfloat16)
    columns = rows_all
    both = lax.psum_scatter(
        jnp.concatenate(
            [
                jnp.dot(columns.T, pre_grad, preferred_element_type=jnp.float32),
                jnp.dot(grad_rows.T, hidden, preferred_element_type=jnp.float32),
            ],
            axis=1,
        ).astype(jnp.bfloat16),
        "fs",
        scatter_dimension=0,
        tiled=True,
    ).astype(jnp.float32)
    up_grad = both[:, :width]
    down_grad = both[:, width:].T
    up_grad, down_grad = (up_grad, down_grad)
    return (input_grad, up_grad, down_grad)


def solution(mesh):
    placed = (
        P(("fs", "tp"), None),
        P("fs", "tp"),
        P(("fs", "tp"), None),
        P("fs", "tp"),
        P("tp", "fs"),
    )
    return jax.shard_map(
        local,
        mesh=mesh,
        in_specs=placed,
        out_specs=(P(("fs", "tp"), None), P("fs", "tp"), P("tp", "fs")),
        check_vma=False,
    )
```

profile of v0, /device:TPU:0, one launch (start us, length us, event | category | flops | bytes accessed | tf_op | source)
XLA Modules:
  0.0 292.9 jit_solution(11470290909760394026)
XLA Ops:
  7.2 0.0 all-gather.4.cloned.1.call-start
  7.2 2.7 pad_maximum_fusion.1
  9.9 0.0 all-gather.4.cloned.1.call-update
  9.9 0.0 all-gather.6.cloned.1.call-start
  10.0 0.7 all-gather.6.cloned.1.call-update
  10.7 0.0 all-gather.8.cloned.1.call-start
  10.7 0.7 all-gather.8.cloned.1.call-update
  11.4 0.0 copy-start.1
  11.4 0.0 reduce-scatter.4.cloned.1.call-start
  11.5 68.3 %all-gather.4.cloned.1.call-done = bf16[1536,4096]{1,0:T(8,128)(2,1)} async-done(((bf16[192,4096]{1,0:T(8,128)(2,1)}), bf16[1536,4096]{1,0:T(8,128)(2,1)}) %all-gather.4.cloned.1.call-update) | async-done | bytes 12582928 | tf_op jit(solution)/shard_map/all_gather | solution.py:13
  79.8 11.6 %fusion.8 = bf16[2048,1024]{0,1:T(8,128)(2,1)} fusion(bf16[1536,4096]{1,0:T(8,128)(2,1)} %all-gather.4.cloned.1.call-done, bf16[1536,1024]{1,0:T(8,128)(2,1)} %param.6), kind=kOutput, calls=%fused_computation.11 | convolution fusion | flops 6450839552 | bytes 13631488 | tf_op jit(solution)/shard_map/dot_general | solution.py:52
  91.4 47.9 %all-gather.6.cloned.1.call-done = bf16[1024,2048]{1,0:T(8,128)(2,1)} async-done(((bf16[1024,128]{1,0:T(8,128)(2,1)}), bf16[1024,2048]{1,0:T(8,128)(2,1)}) %all-gather.6.cloned.1.call-update) | async-done | bytes 4194320 | tf_op jit(solution)/shard_map/all_gather | solution.py:35
  139.4 0.0 copy-done.1
  139.4 0.0 copy-start
  139.4 10.3 %multiply_convert_fusion.1 = bf16[1536,1024]{1,0:T(8,128)(2,1)S(1)} fusion(bf16[1536,1024]{1,0:T(8,128)(2,1)S(1)} %copy-done.1, bf16[1024,2048]{1,0:T(8,128)(2,1)} %all-gather.6.cloned.1.call-done, bf16[1536,4096]{1,0:T(8,128)(2,1)} %all-gather.4.cloned.1.call-done), kind=kOutput, calls=%fused_computation.5 | convolution fusion | flops 6450315264 | bytes 16777216 | tf_op jit(solution)/shard_map/dot_general | solution.py:33
  149.6 0.0 copy-start.2
  149.6 1.7 copy-done.2
  151.3 0.0 copy-done
  151.3 8.4 %fusion.11 = bf16[2048,1024]{0,1:T(8,128)(2,1)} fusion(bf16[1536,1024]{1,0:T(8,128)(2,1)S(1)} %multiply_convert_fusion.1, bf16[1536,4096]{1,0:T(8,128)(2,1)S(1)} %copy-done), kind=kOutput, calls=%fused_computation.12 | convolution fusion | flops 6444548096 | bytes 13631488 | tf_op jit(solution)/shard_map/dot_general | solution.py:51
  159.7 8.5 %pad_maximum_fusion = bf16[2048,2048]{0,1:T(8,128)(2,1)} fusion(bf16[2048,1024]{0,1:T(8,128)(2,1)} %fusion.8, bf16[2048,1024]{0,1:T(8,128)(2,1)} %fusion.11), kind=kLoop, calls=%fused_computation | loop fusion | flops 16777216 | bytes 16777216 | tf_op jit(solution)/shard_map/concatenate | solution.py:49
  168.2 12.3 %copy.10 = bf16[2048,2048]{1,0:T(8,128)(2,1)} copy(bf16[2048,2048]{0,1:T(8,128)(2,1)} %pad_maximum_fusion) | data formatting | bytes 16777216
  180.5 0.0 copy-start.3
  180.5 0.0 reduce-scatter.4.cloned.1.call-update
  180.5 11.8 %all-gather.8.cloned.1.call-done = bf16[2048,1024]{1,0:T(8,128)(2,1)} async-done(((bf16[128,1024]{1,0:T(8,128)(2,1)}), bf16[2048,1024]{1,0:T(8,128)(2,1)}) %all-gather.8.cloned.1.call-update) | async-done | bytes 4194320 | tf_op jit(solution)/shard_map/all_gather | solution.py:41
  192.3 0.0 copy-done.3
  192.3 9.3 %convolution_convert_fusion = bf16[1536,2048]{1,0:T(8,128)(2,1)S(1)} fusion(bf16[1536,1024]{1,0:T(8,128)(2,1)S(1)} %copy-done.3, bf16[2048,1024]{1,0:T(8,128)(2,1)} %all-gather.8.cloned.1.call-done), kind=kOutput, calls=%fused_computation.1 | convolution fusion | flops 6445596672 | bytes 13631488 | tf_op jit(solution)/shard_map/dot_general | solution.py:39
  201.6 76.3 %all_to_all.5 = bf16[8,192,2048]{2,1,0:T(8,128)(2,1)} all-to-all(bf16[8,192,2048]{2,1,0:T(8,128)(2,1)S(1)} %bitcast.8), channel_id=1, replica_groups=mesh['fs'=16,'tp'=8] {'tp'}, dimensions={0} | all-to-all | bytes 12582912 | tf_op jit(solution)/shard_map/all_to_all | solution.py:23
  277.9 5.2 %reduce_sum.12 = bf16[192,2048]{1,0:T(8,128)(2,1)} reduce(bf16[8,192,2048]{2,1,0:T(8,128)(2,1)} %all_to_all.5, bf16[]{:T(256)} %constant.6.clone.1), dimensions={0}, to_apply=%region_0.0 | reduce | flops 2752512 | bytes 7077890 | tf_op jit(solution)/shard_map/reduce_sum | solution.py:24
  283.1 1.3 copy.11
  284.4 0.1 convert_element_type.24
  284.5 0.8 slice_bitcast_fusion
  285.4 1.0 copy.9
  (2 shorter events, 0.0 us)
Async XLA Ops:
  7.2 72.7 %all-gather.4.cloned.1.call-start = ((), (), s32[]{:S(2)}) async-start(), calls=%async_computation.2 | async-start | bytes 14155776 | tf_op jit(solution)/shard_map/all_gather | solution.py:13
  9.9 129.4 %all-gather.6.cloned.1.call-start = ((), (), s32[]{:S(2)}) async-start(), calls=%async_computation.3 | async-start | bytes 4456448 | tf_op jit(solution)/shard_map/all_gather | solution.py:35
  10.7 181.6 %all-gather.8.cloned.1.call-start = ((), (), s32[]{:S(2)}) async-start(), calls=%async_computation.4 | async-start | bytes 4456448 | tf_op jit(solution)/shard_map/all_gather | solution.py:41
  11.4 127.9 %copy-start.1 = (bf16[1536,1024]{1,0:T(8,128)(2,1)S(1)}, bf16[1536,1024]{1,0:T(8,128)(2,1)}, u32[]{:S(2)}) copy-start(bf16[1536,1024]{1,0:T(8,128)(2,1)} %param.6) | copy-start | bytes 9437188
  11.4 271.7 %reduce-scatter.4.cloned.1.call-start = ((), (), s32[]{:S(2)}) async-start(), calls=%async_computation.5 | async-start | bytes 8912896
  139.4 12.0 %copy-start = (bf16[1536,4096]{1,0:T(8,128)(2,1)S(1)}, bf16[1536,4096]{1,0:T(8,128)(2,1)}, u32[]{:S(2)}) copy-start(bf16[1536,4096]{1,0:T(8,128)(2,1)} %all-gather.4.cloned.1.call-done) | copy-start | bytes 37748740
  149.6 1.7 copy-start.2
  180.5 11.8 %copy-start.3 = (bf16[1536,1024]{1,0:T(8,128)(2,1)S(1)}, bf16[1536,1024]{1,0:T(8,128)(2,1)}, u32[]{:S(2)}) copy-start(bf16[1536,1024]{1,0:T(8,128)(2,1)} %copy-done.2) | copy-start | bytes 9437188
Sparse Core Ops, SparseCore 0:
  10.1 69.7 all-gather.3
  81.9 57.3 all-gather.5
  141.5 50.7 all-gather.7
  195.5 85.8 reduce-scatter.3
where the time goes:
time: 294 us; the launch traced here: 293 us
  waiting for transfers between devices  129 us (44%)
  blocking collectives  76.3 us (26%)
  matrix products  39.6 us (13%)
  local copies, waits for them, and re-layouts  17.2 us (6%)
  other arithmetic  16.4 us (6%)
  between operations  13.8 us (5%)
    all_to_all x1, blocking collectives, sum_at_owner(): lax.all_to_all(tiles, axis, split_axis=0, concat_axis=0, tiled=True)  76.3 us
    all_gather x1, waiting for transfers between devices, sent_together(): lax.all_gather(both, axis, axis=dim, tiled=True)  68.3 us
    all_gather x1, waiting for transfers between devices, local(): lax.all_gather(down_weight, 'fs', axis=1, tiled=True)  47.9 us
    unnamed x11, local copies, waits for them, and re-layouts  16.3 us
    all_gather x1, waiting for transfers between devices, local(): lax.all_gather(up_weight, 'fs', axis=0, tiled=True)  11.8 us
    dot_general x1, matrix products, local(): jnp.dot(grad_rows.T, hidden, preferred_element_type=jnp.float32)  11.6 us
    dot_general x1, matrix products, local(): jnp.dot(columns, lax.all_gather(down_weight, 'fs', axis=1, tiled=True).T,...  10.3 us
    dot_general x1, matrix products, local(): jnp.dot(pre_grad, lax.all_gather(up_weight, 'fs', axis=0, tiled=True).T,...  9.33 us
  transfers between devices with their start and end apart: 4, of which 3 were waited for; matrix products, arithmetic and copies ran while one was open for 22% of the time, Pallas kernels for 0%

commit v1 on v0

v1 whole, which is shorter than its diff:
```python
import jax
import jax.numpy as jnp
from jax import lax
from jax.experimental import pallas as pl
from jax.experimental.pallas import tpu as pltpu
from jax.sharding import PartitionSpec as P

MESH = pl.DeviceIdType.MESH
F32 = jnp.float32
BF16 = jnp.bfloat16
SEMS = 160


def rem4(value):
    return lax.rem(value, 4)


def nt(a, b):
    return lax.dot_general(a, b, (((1,), (1,)), ((), ())), preferred_element_type=F32)


def nn(a, b):
    return jnp.dot(a, b, preferred_element_type=F32)


class Wires:
    def __init__(self, send_sem, recv_sem, partner):
        self.send_sem, self.recv_sem, self.partner = send_sem, recv_sem, partner
        self.numbers, self.sent = {}, []

    def number(self, key):
        return self.numbers.setdefault(key, len(self.numbers))

    def copy(self, k, src, dst, device):
        return pltpu.make_async_remote_copy(
            src_ref=src,
            dst_ref=dst,
            send_sem=self.send_sem.at[k],
            recv_sem=self.recv_sem.at[k],
            device_id=device,
            device_id_type=MESH,
        )

    def send(self, key, src, dst, device):
        k = self.number(key)
        self.copy(k, src(), dst(), device).start()
        self.sent.append((key, src))

    def recv(self, key, ref):
        self.copy(self.number(key), ref(), ref(), self.partner).wait_recv()

    def drain(self, tag=None):
        for key, src in self.sent:
            if tag is None or key[0] == tag:
                k = self.number(key)
                self.copy(k, src(), src(), self.partner).wait_send()
        self.sent = [s for s in self.sent if not (tag is None or s[0][0] == tag)]


class Gather:
    def __init__(self, wires, tag, pos, right, left, piece):
        self.w, self.tag, self.pos = wires, tag, pos
        self.right, self.left, self.piece = right, left, piece

    def at(self, hop, p):
        return lambda: self.piece(rem4(self.pos + hop), p)

    def put(self, name, hop, p, device):
        self.w.send((self.tag, name), self.at(hop, p), self.at(hop, p), device)

    def got(self, name, hop, p):
        self.w.recv((self.tag, name), self.at(hop, p))

    def own(self):
        self.put("R0", 0, 0, self.right)
        self.put("L0", 0, 1, self.left)
        self.put("R1", 0, 1, self.right)
        self.put("L1", 0, 0, self.left)

    def forward(self):
        self.got("R0", 3, 0)
        self.put("R2", 3, 0, self.right)
        self.got("L0", 1, 1)
        self.put("L2", 1, 1, self.left)

    def near(self):
        self.got("R1", 3, 1)
        self.got("L1", 1, 0)

    def far(self):
        self.got("R2", 2, 0)
        self.got("L2", 2, 1)


class Scatter:
    def __init__(self, wires, tag, pos, right, left, piece, landing):
        self.w, self.tag, self.pos = wires, tag, pos
        self.right, self.left = right, left
        self.piece, self.landing = piece, landing

    def at(self, hop, p):
        return lambda: self.piece(rem4(self.pos + hop), p)

    def put(self, side, m, hop, p):
        self.w.send(
            (self.tag, side, m),
            self.at(hop, p),
            lambda: self.landing(side, m),
            self.right if side == 0 else self.left,
        )

    def got(self, side, m):
        self.w.recv((self.tag, side, m), lambda: self.landing(side, m))
        return self.landing(side, m)

    def far(self):
        self.put(0, 0, 2, 0)
        self.put(1, 0, 2, 1)

    def to_right(self):
        self.put(0, 1, 1, 1)

    def to_left(self):
        self.put(1, 1, 3, 0)

    def middle(self):
        for side, hop, p in ((0, 1, 0), (1, 3, 1)):
            came = self.got(side, 0)
            mine = self.at(hop, p)()
            mine[...] = (mine[...].astype(F32) + came[...].astype(F32)).astype(BF16)
            self.put(side, 2, hop, p)

    def finish(self, out=None):
        for p, a, b in ((1, (0, 1), (1, 2)), (0, (1, 1), (0, 2))):
            first, second = self.got(*a), self.got(*b)
            mine = self.at(0, p)()
            total = mine[...].astype(F32) + first[...].astype(F32) + second[...].astype(F32)
            target = mine if out is None else out(p)
            target[...] = total.astype(target.dtype)


def kernel(
    ni_hbm, pa_hbm, og_hbm, uw_hbm, dw_hbm,
    ig_hbm, ug_hbm, dg_hbm,
    ni, og, wd, wu, pg, ht, pgt, part, gd, gu,
    cross, xland, zland_d, yland_d, yone_d, zone_d,
    zland_u, yland_u, yone_u, zone_u,
    dg, ug, send_sem, recv_sem, local_sem,
):
    fs, tp = lax.axis_index("fs"), lax.axis_index("tp")
    z, y, x, c = fs // 4, rem4(fs), tp // 2, lax.rem(tp, 2)
    x_right = {"fs": fs, "tp": rem4(x + 1) * 2 + c}
    x_left = {"fs": fs, "tp": rem4(x + 3) * 2 + c}
    y_right = {"fs": z * 4 + rem4(y + 1), "tp": tp}
    y_left = {"fs": z * 4 + rem4(y + 3), "tp": tp}
    z_right = {"fs": rem4(z + 1) * 4 + y, "tp": tp}
    z_left = {"fs": rem4(z + 3) * 4 + y, "tp": tp}
    partner = {"fs": fs, "tp": x * 2 + 1 - c}

    rows = og_hbm.shape[0]
    half = rows // 2
    ff, cols = dw_hbm.shape
    wide = 4 * cols
    quarter = ff // 4
    urows = uw_hbm.shape[0]
    tokens = pg.shape[0]

    w = Wires(send_sem, recv_sem, partner)

    def token_rows(ref, block):
        return ref.at[pl.ds(pl.multiple_of(block * rows, rows), rows), :]

    def lanes(i):
        return pl.ds(pl.multiple_of(i * cols, cols), cols)

    mine = [
        (dw_hbm, wd.at[z, :, lanes(y)]),
        (og_hbm, token_rows(og, tp)),
        (uw_hbm, wu.at[z, y]),
        (pa_hbm, pg),
        (ni_hbm, token_rows(ni, tp)),
    ]
    local = [
        pltpu.make_async_copy(src, dst, local_sem.at[i])
        for i, (src, dst) in enumerate(mine)
    ]
    for copy in local:
        copy.start()

    barrier = pltpu.get_barrier_semaphore()
    for device in (x_right, x_left, y_right, y_left, z_right, z_left, partner):
        pl.semaphore_signal(barrier, inc=1, device_id=device, device_id_type=MESH)
    pl.semaphore_wait(barrier, 7)

    def wd_rows(p):
        return pl.ds(p * quarter, quarter)

    def wu_rows(p):
        return pl.ds(p * (urows // 4), urows // 4)

    def weight_rings(tag, one, z_group, y_group):
        return (
            (
                Gather(w, tag + "a1", y, y_right, y_left, lambda i, p: one(z, i, p)),
                Gather(w, tag + "b1", z, z_right, z_left, lambda i, p: one(i, y, 2 + p)),
            ),
            (
                Gather(w, tag + "a2", z, z_right, z_left, lambda i, p: z_group(i, p)),
                Gather(w, tag + "b2", y, y_right, y_left, lambda i, p: y_group(i, 2 + p)),
            ),
        )

    wd1, wd2 = weight_rings(
        "d",
        lambda zi, yi, p: wd.at[zi, wd_rows(p), lanes(yi)],
        lambda zi, p: wd.at[zi, wd_rows(p), :],
        lambda yi, p: wd.at[:, wd_rows(p), lanes(yi)],
    )
    wu1, wu2 = weight_rings(
        "u",
        lambda zi, yi, p: wu.at[zi, yi, wu_rows(p), :],
        lambda zi, p: wu.at[zi, :, wu_rows(p), :],
        lambda yi, p: wu.at[:, yi, wu_rows(p), :],
    )

    def token_piece(ref, core):
        def piece(i, p):
            start = pl.multiple_of((i * 2 + core) * rows + p * half, half)
            return ref.at[pl.ds(start, half), :]

        return piece

    rings = {
        "o": Gather(w, "o", x, x_right, x_left, token_piece(og, c)),
        "n": Gather(w, "n", x, x_right, x_left, token_piece(ni, c)),
    }
    others = {"o": token_piece(og, 1 - c), "n": token_piece(ni, 1 - c)}

    def hand(tag, *pieces):
        for hop, p in pieces:
            ref = rings[tag].at(hop, p)
            w.send((tag, "c", hop, p), ref, ref, partner)

    def handed(tag):
        for hop in range(4):
            for p in range(2):
                w.recv((tag, "c", hop, p), lambda: others[tag](rem4(x + hop), p))

    def token_own(tag):
        rings[tag].own()
        hand(tag, (0, 0), (0, 1))

    def token_forward(tag):
        rings[tag].forward()
        hand(tag, (3, 0), (1, 1))

    def token_near(tag):
        rings[tag].near()
        hand(tag, (3, 1), (1, 0))

    def token_far(tag):
        rings[tag].far()
        hand(tag, (2, 0), (2, 1))

    def each(pair, step):
        for ring in pair:
            getattr(ring, step)()

    def hidden(count, first):
        def body(j, carry):
            at = pl.multiple_of(j * 128, 128)
            active = jnp.maximum(pg[pl.ds(at, 128), :].astype(F32), 0.0)
            ht[:, pl.ds(at, 128)] = (active * active).astype(BF16).T
            return carry

        lax.fori_loop(first, first + count, body, 0)

    local[0].wait()
    each(wd1, "own")
    local[1].wait()
    token_own("o")
    local[3].wait()
    hidden(3, 0)
    each(wd1, "forward")
    local[2].wait()
    each(wu1, "own")
    hidden(3, 3)
    each(wd1, "near")
    each(wd1, "far")
    each(wu1, "forward")
    each(wd2, "own")
    hidden(3, 6)
    token_forward("o")
    local[4].wait()
    token_own("n")
    each(wu1, "near")
    each(wu1, "far")
    hidden(3, 9)
    each(wd2, "forward")
    each(wu2, "own")
    token_near("o")
    each(wd2, "near")
    each(wd2, "far")
    token_far("o")
    handed("o")

    block = 256

    def pre_grad(i, carry):
        at = pl.ds(pl.multiple_of(i * block, block), block)
        weight = jnp.concatenate([wd[k] for k in range(4)], axis=1)
        grad = nt(og[at, :], weight)
        active = jnp.maximum(pg[at, :].astype(F32), 0.0)
        value = (2.0 * active * grad).astype(BF16)
        pg[at, :] = value
        pgt[:, at] = value.T

        @pl.when(i == 2)
        def _():
            each(wu2, "forward")

        @pl.when(i == 4)
        def _():
            token_forward("n")

        return carry

    lax.fori_loop(0, tokens // block, pre_grad, 0)

    def grad_rings(tag, grad, zland, yland, yone, zone):
        return (
            (
                Scatter(
                    w, tag + "a1", z, z_right, z_left,
                    lambda i, p: grad.at[i, wd_rows(p), :],
                    lambda side, m: zland.at[side, m],
                ),
                Scatter(
                    w, tag + "b1", y, y_right, y_left,
                    lambda i, p: grad.at[:, wd_rows(2 + p), lanes(i)],
                    lambda side, m: yland.at[side, m],
                ),
            ),
            (
                Scatter(
                    w, tag + "a2", y, y_right, y_left,
                    lambda i, p: grad.at[z, wd_rows(p), lanes(i)],
                    lambda side, m: yone.at[side, m],
                ),
                Scatter(
                    w, tag + "b2", z, z_right, z_left,
                    lambda i, p: grad.at[i, wd_rows(2 + p), lanes(y)],
                    lambda side, m: zone.at[side, m],
                ),
            ),
        )

    gd1, gd2 = grad_rings("D", gd, zland_d, yland_d, yone_d, zone_d)
    gu1, gu2 = grad_rings("U", gu, zland_u, yland_u, yone_u, zone_u)
    upper = ff // 2

    def hop_of(k):
        return jnp.where(k == 0, 2, jnp.where(k == 1, 1, jnp.where(k == 2, 3, 0)))

    def weight_grad(left, right, grad, first, extra):
        def body(k, carry):
            zi, yi = rem4(z + hop_of(k)), rem4(y + hop_of(k))
            strip = right[:, pl.ds(pl.multiple_of(zi * wide, wide), wide)]
            grad[zi, :upper, :] = nn(left[:upper, :], strip).astype(BF16)
            strip = jnp.concatenate(
                [right[:, pl.ds(pl.multiple_of(g * wide + yi * cols, cols), cols)] for g in range(4)],
                axis=1,
            )
            value = nn(left[upper:, :], strip).astype(BF16)
            for g in range(4):
                grad[g, upper:, lanes(yi)] = value[:, g * cols : (g + 1) * cols]

            for turn, step in ((0, "far"), (1, "to_right"), (2, "to_left")):

                @pl.when(k == turn)
                def _(step=step):
                    each(first, step)

            extra(k)
            return carry

        lax.fori_loop(0, 4, body, 0)

    def while_down(k):
        @pl.when(k == 2)
        def _():
            token_near("n")

    weight_grad(ht, og, gd, gd1, while_down)

    each(wu2, "near")
    each(wu2, "far")

    def share(block):
        return part.at[block]

    xs = Scatter(
        w, "x", x, x_right, x_left,
        lambda i, p: part.at[i * 2 + c, pl.ds(p * half, half), :],
        lambda side, m: xland.at[side, m],
    )
    cross_base = w.number(("cross", 0))
    for k in range(1, 4):
        w.number(("cross", k))

    def product(index):
        at = pl.ds(pl.multiple_of(index * rows, rows), rows)
        weight = wu[...].reshape(16 * urows, ff)
        part[index] = nt(pg[at, :], weight).astype(BF16)

    def add_cross(k):
        index = rem4(x + hop_of(k)) * 2 + c
        w.copy(cross_base + k, cross.at[k], cross.at[k], partner).wait_recv()
        total = part[index].astype(F32) + cross[k].astype(F32)
        part[index] = total.astype(BF16)

    def input_grad(k, carry):
        xi = rem4(x + hop_of(k))
        product(xi * 2 + 1 - c)
        w.copy(cross_base + k, part.at[xi * 2 + 1 - c], cross.at[k], partner).start()

        @pl.when(k > 0)
        def _():
            add_cross(k - 1)

        for turn, step in ((1, xs.far), (2, xs.to_right), (3, xs.to_left)):

            @pl.when(k == turn)
            def _(step=step):
                step()

        product(xi * 2 + c)

        @pl.when(k == 1)
        def _():
            token_far("n")

        @pl.when(k == 2)
        def _():
            each(gd1, "middle")

        return carry

    lax.fori_loop(0, 4, input_grad, 0)
    add_cross(3)
    handed("n")

    def while_up(k):
        @pl.when(k == 2)
        def _():
            xs.middle()

        @pl.when(k == 3)
        def _():
            each(gd1, "finish")
            each(gd2, "far")
            each(gd2, "to_right")
            each(gd2, "to_left")

    weight_grad(pgt, ni, gu, gu1, while_up)

    each(gu1, "middle")
    each(gd2, "middle")

    def own_rows(out):
        return (
            lambda p: out.at[wd_rows(p), :],
            lambda p: out.at[wd_rows(2 + p), :],
        )

    for ring, out in zip(gd2, own_rows(dg)):
        ring.finish(out)
    down_out = pltpu.make_async_copy(dg, dg_hbm, local_sem.at[5])
    down_out.start()
    w.drain("o")
    ig = og.at[pl.ds(0, rows), :]
    xs.finish(lambda p: og.at[pl.ds(p * half, half), :])
    input_out = pltpu.make_async_copy(ig, ig_hbm, local_sem.at[6])
    input_out.start()
    each(gu1, "finish")
    each(gu2, "far")
    each(gu2, "to_right")
    each(gu2, "to_left")
    each(gu2, "middle")
    for ring, out in zip(gu2, own_rows(ug)):
        ring.finish(out)
    up_out = pltpu.make_async_copy(ug, ug_hbm, local_sem.at[7])
    up_out.start()
    for k in range(4):
        w.copy(cross_base + k, cross.at[k], cross.at[k], partner).wait_send()
    w.drain()
    down_out.wait()
    input_out.wait()
    up_out.wait()


def local(normed_input, pre_act, out_grad, up_weight, down_weight):
    rows, d = out_grad.shape
    tokens, ff = pre_act.shape
    cols = down_weight.shape[1]
    quarter = ff // 4
    half = rows // 2
    grads = [
        pltpu.VMEM((2, 3, quarter, 4 * cols), BF16),
        pltpu.VMEM((2, 3, 4, quarter, cols), BF16),
        pltpu.VMEM((2, 3, quarter, cols), BF16),
        pltpu.VMEM((2, 3, quarter, cols), BF16),
    ]
    input_grad, up_grad, down_grad = pl.pallas_call(
        kernel,
        out_shape=(
            jax.ShapeDtypeStruct((rows, d), BF16),
            jax.ShapeDtypeStruct((ff, cols), F32),
            jax.ShapeDtypeStruct((ff, cols), F32),
        ),
        in_specs=[pl.BlockSpec(memory_space=pl.ANY)] * 5,
        out_specs=(pl.BlockSpec(memory_space=pl.ANY),) * 3,
        scratch_shapes=[
            pltpu.VMEM((tokens, d), BF16),
            pltpu.VMEM((tokens, d), BF16),
            pltpu.VMEM((4, ff, 4 * cols), BF16),
            pltpu.VMEM((4, 4, d // 16, ff), BF16),
            pltpu.VMEM((tokens, ff), BF16),
            pltpu.VMEM((ff, tokens), BF16),
            pltpu.VMEM((ff, tokens), BF16),
            pltpu.VMEM((8, rows, d), BF16),
            pltpu.VMEM((4, ff, 4 * cols), BF16),
            pltpu.VMEM((4, ff, 4 * cols), BF16),
            pltpu.VMEM((4, rows, d), BF16),
            pltpu.VMEM((2, 3, half, d), BF16),
            *grads,
            *grads,
            pltpu.VMEM((ff, cols), F32),
            pltpu.VMEM((ff, cols), F32),
            pltpu.SemaphoreType.DMA((SEMS,)),
            pltpu.SemaphoreType.DMA((SEMS,)),
            pltpu.SemaphoreType.DMA((8,)),
        ],
        compiler_params=pltpu.CompilerParams(
            collective_id=0,
            has_side_effects=True,
            vmem_limit_bytes=67043328,
        ),
        name="ffn_backward",
    )(normed_input, pre_act, out_grad, up_weight, down_weight)
    return input_grad, up_grad.T, down_grad


def solution(mesh):
    placed = (
        P(("fs", "tp"), None),
        P("fs", "tp"),
        P(("fs", "tp"), None),
        P("fs", "tp"),
        P("tp", "fs"),
    )
    return jax.shard_map(
        local,
        mesh=mesh,
        in_specs=placed,
        out_specs=(P(("fs", "tp"), None), P("fs", "tp"), P("tp", "fs")),
        check_vma=False,
    )
```

time: 294 us -> 114 us (0.39)
  waiting for transfers between devices: 129 us -> 0 us
  Pallas kernels: 0 us -> 107 us
  blocking collectives: 76.3 us -> 0 us
  matrix products: 39.6 us -> 0 us
  other arithmetic: 16.4 us -> 0 us
  between operations: 13.8 us -> 0.64 us
  local copies, waits for them, and re-layouts: 17.2 us -> 5.99 us
    all_gather x3 -> x0, waiting for transfers between devices: 128 us -> none  [the longest x1 68.3 us: sent_together(): lax.all_gather(both, axis, axis=dim, tiled=True)]
    pallas_call x0 -> x1, Pallas kernels: none -> 107 us  [local(): pl.pallas_call(kernel, out_shape=(jax.ShapeDtypeStruct((rows, d), BF16),...]
    all_to_all x1 -> x0, blocking collectives: 76.3 us -> none  [sum_at_owner(): lax.all_to_all(tiles, axis, split_axis=0, concat_axis=0, tiled=True)]
    dot_general x4 -> x0, matrix products: 39.6 us -> none  [the longest x1 11.6 us: local(): jnp.dot(grad_rows.T, hidden, preferred_element_type=jnp.float32)]
    concatenate x2 -> x0, other arithmetic: 11.2 us -> none  [the longest x1 8.45 us: local(): jnp.concatenate([jnp.dot(columns.T, pre_grad, preferred_element_type=jnp....]
    unnamed x11 -> x3, local copies, waits for them, and re-layouts: 16.3 us -> 5.99 us
    reduce_sum x1 -> x0, other arithmetic: 5.16 us -> none  [sum_at_owner(): return arrived.astype(jnp.float32).sum(axis=0)]
  transfers between devices with their start and end apart: 4 -> 0, of which waited for: 3 -> 0; matrix products, arithmetic and copies ran while one was open for 22% -> 0% of each run, Pallas kernels for 0% -> 0%
where the time goes in v1:
time: 114 us
  Pallas kernels  107 us (94%)
  local copies, waits for them, and re-layouts  5.99 us (5%)
    pallas_call x1, Pallas kernels, local(): pl.pallas_call(kernel, out_shape=(jax.ShapeDtypeStruct((rows, d), BF16),...  107 us
    unnamed x3, local copies, waits for them, and re-layouts  5.99 us

profile of v1, /device:TPU:0, one launch (start us, length us, event | category | flops | bytes accessed | tf_op | source)
XLA Modules:
  0.0 113.5 jit_solution(3674089991197157067)
XLA Ops:
  0.6 106.9 %ffn_backward.1 = (bf16[192,2048]{1,0:T(8,128)(2,1)}, f32[1024,128]{1,0:T(8,128)}, f32[1024,128]{1,0:T(8,128)}) custom-call(bf16[192,2048]{1,0:T(8,128)(2,1)} %ni_hbm.1, bf16[1536,1024]{1,0:T(8,128)(2,1)} %pa_hbm.1, bf16[192,2048]{1,0:T(8,128)(2,1)} %og_hbm.1, bf16[128,1024]{1,0:T(8,128)(2,1)} %uw_hbm.1, bf16[1024,128]{1,0:T(8,128)(2,1)} %dw_hbm.1), custom_call_target="tpu_custom_call" | custom-call | tf_op jit(solution)/shard_map/ffn_backward/pallas_call | solution.py:514
  107.6 2.0 %copy.8 = f32[128,1024]{1,0:T(8,128)} copy(f32[128,1024]{0,1:T(8,128)} %bitcast.1) | data formatting | bytes 1048576
  109.6 2.1 %copy.11 = bf16[192,2048]{1,0:T(8,128)(2,1)} copy(bf16[192,2048]{1,0:T(8,128)(2,1)} %get-tuple-element.15) | data formatting | bytes 1572864
  111.7 1.9 %copy.12 = f32[1024,128]{1,0:T(8,128)} copy(f32[1024,128]{1,0:T(8,128)} %get-tuple-element.17) | data formatting | bytes 1048576

commit v2 on v1

--- a/solution.py
+++ b/solution.py
@@ -1,3 +1,5 @@
+import math
+
 import jax
 import jax.numpy as jnp
 from jax import lax
@@ -8,7 +10,7 @@
 MESH = pl.DeviceIdType.MESH
 F32 = jnp.float32
 BF16 = jnp.bfloat16
-SEMS = 160
+SENDS, RECVS = 8, 64
 
 
 def rem4(value):
@@ -23,120 +25,165 @@
     return jnp.dot(a, b, preferred_element_type=F32)
 
 
+def size_of(ref):
+    return 2 * math.prod(ref.shape)
+
+
 class Wires:
-    def __init__(self, send_sem, recv_sem, partner):
+    def __init__(self, send_sem, recv_sem, partner, filler):
         self.send_sem, self.recv_sem, self.partner = send_sem, recv_sem, partner
-        self.numbers, self.sent = {}, []
-
-    def number(self, key):
-        return self.numbers.setdefault(key, len(self.numbers))
-
-    def copy(self, k, src, dst, device):
+        self.filler = filler
+        self.groups, self.keys, self.bytes = {}, {}, {}
+
+    def group(self, name):
+        return self.groups.setdefault(name, len(self.groups))
+
+    def key(self, name):
+        return self.keys.setdefault(name, len(self.keys))
+
+    def copy(self, g, k, src, dst, device):
         return pltpu.make_async_remote_copy(
             src_ref=src,
             dst_ref=dst,
-            send_sem=self.send_sem.at[k],
+            send_sem=self.send_sem.at[g],
             recv_sem=self.recv_sem.at[k],
             device_id=device,
             device_id_type=MESH,
         )
 
-    def send(self, key, src, dst, device):
-        k = self.number(key)
-        self.copy(k, src(), dst(), device).start()
-        self.sent.append((key, src))
-
-    def recv(self, key, ref):
-        self.copy(self.number(key), ref(), ref(), self.partner).wait_recv()
-
-    def drain(self, tag=None):
-        for key, src in self.sent:
-            if tag is None or key[0] == tag:
-                k = self.number(key)
-                self.copy(k, src(), src(), self.partner).wait_send()
-        self.sent = [s for s in self.sent if not (tag is None or s[0][0] == tag)]
+    def send(self, group, key, src, dst, device):
+        self.copy(self.group(group), self.key(key), src, dst, device).start()
+        self.bytes[group] = self.bytes.get(group, 0) + size_of(src)
+
+    def recv(self, key, size):
+        ref = self.filler(size)
+        self.copy(0, self.key(key), ref, ref, self.partner).wait_recv()
+
+    def drain(self, group):
+        ref = self.filler(self.bytes[group])
+        self.copy(self.group(group), 0, ref, ref, self.partner).wait_send()
 
 
 class Gather:
-    def __init__(self, wires, tag, pos, right, left, piece):
-        self.w, self.tag, self.pos = wires, tag, pos
+    def __init__(self, wires, group, tag, pos, right, left, piece):
+        self.w, self.group, self.tag, self.pos = wires, group, tag, pos
         self.right, self.left, self.piece = right, left, piece
+        self.size = size_of(piece(pos, 0))
 
     def at(self, hop, p):
-        return lambda: self.piece(rem4(self.pos + hop), p)
+        return self.piece(rem4(self.pos + hop), p)
 
     def put(self, name, hop, p, device):
-        self.w.send((self.tag, name), self.at(hop, p), self.at(hop, p), device)
-
-    def got(self, name, hop, p):
-        self.w.recv((self.tag, name), self.at(hop, p))
+        ref = self.at(hop, p)
+        self.w.send(self.group, (self.tag, name), ref, ref, device)
 
     def own(self):
-        self.put("R0", 0, 0, self.right)
-        self.put("L0", 0, 1, self.left)
-        self.put("R1", 0, 1, self.right)
-        self.put("L1", 0, 0, self.left)
+        self.put("first", 0, 0, self.right)
+        self.put("first", 0, 1, self.left)
+        self.put("near", 0, 1, self.right)
+        self.put("near", 0, 0, self.left)
 
     def forward(self):
-        self.got("R0", 3, 0)
-        self.put("R2", 3, 0, self.right)
-        self.got("L0", 1, 1)
-        self.put("L2", 1, 1, self.left)
+        self.w.recv((self.tag, "first"), 2 * self.size)
+        self.put("far", 3, 0, self.right)
+        self.put("far", 1, 1, self.left)
 
     def near(self):
-        self.got("R1", 3, 1)
-        self.got("L1", 1, 0)
+        self.w.recv((self.tag, "near"), 2 * self.size)
 
     def far(self):
-        self.got("R2", 2, 0)
-        self.got("L2", 2, 1)
+        self.w.recv((self.tag, "far"), 2 * self.size)
+
+
+class QuarterGather(Gather):
+    def __init__(self, wires, group, tag, pos, right, left, piece, quarter):
+        super().__init__(wires, group, tag, pos, right, left, piece)
+        self.quarter = quarter
+
+    def give(self, turn, *members):
+        name = (self.tag, "near" if turn else "first")
+        for h in members:
+            for device, p in ((self.right, turn), (self.left, 1 - turn)):
+                ref = self.quarter(self.pos, p, h)
+                self.w.send(self.group, name, ref, ref, device)
 
 
 class Scatter:
-    def __init__(self, wires, tag, pos, right, left, piece, landing):
-        self.w, self.tag, self.pos = wires, tag, pos
+    def __init__(self, wires, group, tag, pos, right, left, piece, landing):
+        self.w, self.group, self.tag, self.pos = wires, group, tag, pos
         self.right, self.left = right, left
         self.piece, self.landing = piece, landing
+        self.size = size_of(piece(pos, 0))
 
     def at(self, hop, p):
-        return lambda: self.piece(rem4(self.pos + hop), p)
-
-    def put(self, side, m, hop, p):
+        return self.piece(rem4(self.pos + hop), p)
+
+    def put(self, name, side, m, hop, p):
         self.w.send(
-            (self.tag, side, m),
+            self.group,
+            (self.tag, name),
             self.at(hop, p),
-            lambda: self.landing(side, m),
+            self.landing(side, m),
             self.right if side == 0 else self.left,
         )
 
-    def got(self, side, m):
-        self.w.recv((self.tag, side, m), lambda: self.landing(side, m))
-        return self.landing(side, m)
-
     def far(self):
-        self.put(0, 0, 2, 0)
-        self.put(1, 0, 2, 1)
+        self.put("first", 0, 0, 2, 0)
+        self.put("first", 1, 0, 2, 1)
 
     def to_right(self):
-        self.put(0, 1, 1, 1)
+        self.put("last", 0, 1, 1, 1)
 
     def to_left(self):
-        self.put(1, 1, 3, 0)
+        self.put("last", 1, 1, 3, 0)
+
+    def add_first(self):
+        self.w.recv((self.tag, "first"), 2 * self.size)
+        for side, hop, p in ((0, 1, 0), (1, 3, 1)):
+            came, mine = self.landing(side, 0), self.at(hop, p)
+            mine[...] = (mine[...].astype(F32) + came[...].astype(F32)).astype(BF16)
 
     def middle(self):
-        for side, hop, p in ((0, 1, 0), (1, 3, 1)):
-            came = self.got(side, 0)
-            mine = self.at(hop, p)()
-            mine[...] = (mine[...].astype(F32) + came[...].astype(F32)).astype(BF16)
-            self.put(side, 2, hop, p)
+        self.add_first()
+        self.put("last", 0, 2, 1, 0)
+        self.put("last", 1, 2, 3, 1)
 
     def finish(self, out=None):
-        for p, a, b in ((1, (0, 1), (1, 2)), (0, (1, 1), (0, 2))):
-            first, second = self.got(*a), self.got(*b)
-            mine = self.at(0, p)()
+        self.w.recv((self.tag, "last"), 4 * self.size)
+        for p, near, far in ((1, 0, 1), (0, 1, 0)):
+            first, second = self.landing(near, 1), self.landing(far, 2)
+            mine = self.at(0, p)
             total = mine[...].astype(F32) + first[...].astype(F32) + second[...].astype(F32)
             target = mine if out is None else out(p)
             target[...] = total.astype(target.dtype)
+
+
+class QuarterScatter(Scatter):
+    def __init__(self, wires, group, tag, pos, right, left, piece, landing, quarter, landed):
+        super().__init__(wires, group, tag, pos, right, left, piece, landing)
+        self.quarter, self.landed = quarter, landed
+
+    def give(self, *members):
+        for h in members:
+            for side, hop, p in ((0, 1, 0), (1, 3, 1)):
+                self.w.send(
+                    self.group,
+                    (self.tag, h),
+                    self.quarter(rem4(self.pos + hop), p, h),
+                    self.landed(side, 2, h),
+                    self.right if side == 0 else self.left,
+                )
+
+    def settle_near(self):
+        self.w.recv((self.tag, "last"), 2 * self.size)
+
+    def settle(self, h):
+        self.w.recv((self.tag, h), self.size // 2)
+        for p, near, far in ((1, 0, 1), (0, 1, 0)):
+            first, second = self.landed(near, 1, h), self.landed(far, 2, h)
+            mine = self.quarter(self.pos, p, h)
+            total = mine[...].astype(F32) + first[...].astype(F32) + second[...].astype(F32)
+            mine[...] = total.astype(BF16)
 
 
 def kernel(
@@ -165,7 +212,8 @@
     urows = uw_hbm.shape[0]
     tokens = pg.shape[0]
 
-    w = Wires(send_sem, recv_sem, partner)
+    line = 2 * og.shape[1]
+    w = Wires(send_sem, recv_sem, partner, lambda size: og.at[pl.ds(0, size // line), :])
 
     def token_rows(ref, block):
         return ref.at[pl.ds(pl.multiple_of(block * rows, rows), rows), :]
@@ -201,20 +249,32 @@
     def weight_rings(tag, one, z_group, y_group):
         return (
             (
-                Gather(w, tag + "a1", y, y_right, y_left, lambda i, p: one(z, i, p)),
-                Gather(w, tag + "b1", z, z_right, z_left, lambda i, p: one(i, y, 2 + p)),
+                Gather(w, tag, tag + "a1", y, y_right, y_left, lambda i, p: one(z, i, p)),
+                Gather(w, tag, tag + "b1", z, z_right, z_left, lambda i, p: one(i, y, 2 + p)),
             ),
             (
-                Gather(w, tag + "a2", z, z_right, z_left, lambda i, p: z_group(i, p)),
-                Gather(w, tag + "b2", y, y_right, y_left, lambda i, p: y_group(i, 2 + p)),
+                Gather(w, tag, tag + "a2", z, z_right, z_left, lambda i, p: z_group(i, p)),
+                Gather(w, tag, tag + "b2", y, y_right, y_left, lambda i, p: y_group(i, 2 + p)),
             ),
         )
 
-    wd1, wd2 = weight_rings(
+    wd1, _ = weight_rings(
         "d",
         lambda zi, yi, p: wd.at[zi, wd_rows(p), lanes(yi)],
         lambda zi, p: wd.at[zi, wd_rows(p), :],
         lambda yi, p: wd.at[:, wd_rows(p), lanes(yi)],
+    )
+    wd2 = (
+        QuarterGather(
+            w, "d", "da2", z, z_right, z_left,
+            lambda i, p: wd.at[i, wd_rows(p), :],
+            lambda i, p, h: wd.at[i, wd_rows(p), lanes(rem4(y + h))],
+        ),
+        QuarterGather(
+            w, "d", "db2", y, y_right, y_left,
+            lambda i, p: wd.at[:, wd_rows(2 + p), lanes(i)],
+            lambda i, p, h: wd.at[rem4(z + h), wd_rows(2 + p), lanes(i)],
+        ),
     )
     wu1, wu2 = weight_rings(
         "u",
@@ -231,20 +291,17 @@
         return piece
 
     rings = {
-        "o": Gather(w, "o", x, x_right, x_left, token_piece(og, c)),
-        "n": Gather(w, "n", x, x_right, x_left, token_piece(ni, c)),
+        "o": Gather(w, "o", "o", x, x_right, x_left, token_piece(og, c)),
+        "n": Gather(w, "n", "n", x, x_right, x_left, token_piece(ni, c)),
     }
-    others = {"o": token_piece(og, 1 - c), "n": token_piece(ni, 1 - c)}
 
     def hand(tag, *pieces):
         for hop, p in pieces:
             ref = rings[tag].at(hop, p)
-            w.send((tag, "c", hop, p), ref, ref, partner)
+            w.send(tag, (tag, "cross"), ref, ref, partner)
 
     def handed(tag):
-        for hop in range(4):
-            for p in range(2):
-                w.recv((tag, "c", hop, p), lambda: others[tag](rem4(x + hop), p))
+        w.recv((tag, "cross"), 8 * rings[tag].size)
 
     def token_own(tag):
         rings[tag].own()
@@ -275,27 +332,33 @@
 
         lax.fori_loop(first, first + count, body, 0)
 
+    def give(pair, *what):
+        for ring in pair:
+            ring.give(*what)
+
     local[0].wait()
     each(wd1, "own")
     local[1].wait()
     token_own("o")
-    local[3].wait()
-    hidden(3, 0)
-    each(wd1, "forward")
     local[2].wait()
     each(wu1, "own")
-    hidden(3, 3)
+    give(wd2, 0, 0)
+    give(wd2, 1, 0)
+    local[3].wait()
+    hidden(6, 0)
+    each(wd1, "forward")
+    each(wu1, "forward")
+    hidden(6, 6)
     each(wd1, "near")
+    give(wd2, 0, 1, 3)
+    token_forward("o")
     each(wd1, "far")
-    each(wu1, "forward")
-    each(wd2, "own")
-    hidden(3, 6)
-    token_forward("o")
+    give(wd2, 0, 2)
+    give(wd2, 1, 1, 3, 2)
     local[4].wait()
     token_own("n")
     each(wu1, "near")
     each(wu1, "far")
-    hidden(3, 9)
     each(wd2, "forward")
     each(wu2, "own")
     token_near("o")
@@ -315,11 +378,11 @@
         pg[at, :] = value
         pgt[:, at] = value.T
 
-        @pl.when(i == 2)
+        @pl.when(i == 3)
         def _():
             each(wu2, "forward")
 
-        @pl.when(i == 4)
+        @pl.when(i == 5)
         def _():
             token_forward("n")
 
@@ -331,24 +394,24 @@
         return (
             (
                 Scatter(
-                    w, tag + "a1", z, z_right, z_left,
+                    w, tag, tag + "a1", z, z_right, z_left,
                     lambda i, p: grad.at[i, wd_rows(p), :],
                     lambda side, m: zland.at[side, m],
                 ),
                 Scatter(
-                    w, tag + "b1", y, y_right, y_left,
+                    w, tag, tag + "b1", y, y_right, y_left,
                     lambda i, p: grad.at[:, wd_rows(2 + p), lanes(i)],
                     lambda side, m: yland.at[side, m],
                 ),
             ),
             (
                 Scatter(
-                    w, tag + "a2", y, y_right, y_left,
+                    w, tag, tag + "a2", y, y_right, y_left,
                     lambda i, p: grad.at[z, wd_rows(p), lanes(i)],
                     lambda side, m: yone.at[side, m],
                 ),
                 Scatter(
-                    w, tag + "b2", z, z_right, z_left,
+                    w, tag, tag + "b2", z, z_right, z_left,
                     lambda i, p: grad.at[i, wd_rows(2 + p), lanes(y)],
                     lambda side, m: zone.at[side, m],
                 ),
@@ -356,7 +419,23 @@
         )
 
     gd1, gd2 = grad_rings("D", gd, zland_d, yland_d, yone_d, zone_d)
-    gu1, gu2 = grad_rings("U", gu, zland_u, yland_u, yone_u, zone_u)
+    _, gu2 = grad_rings("U", gu, zland_u, yland_u, yone_u, zone_u)
+    gu1 = (
+        QuarterScatter(
+            w, "U", "Ua1", z, z_right, z_left,
+            lambda i, p: gu.at[i, wd_rows(p), :],
+            lambda side, m: zland_u.at[side, m],
+            lambda i, p, h: gu.at[i, wd_rows(p), lanes(rem4(y + h))],
+            lambda side, m, h: zland_u.at[side, m, :, lanes(rem4(y + h))],
+        ),
+        QuarterScatter(
+            w, "U", "Ub1", y, y_right, y_left,
+            lambda i, p: gu.at[:, wd_rows(2 + p), lanes(i)],
+            lambda side, m: yland_u.at[side, m],
+            lambda i, p, h: gu.at[rem4(z + h), wd_rows(2 + p), lanes(i)],
+            lambda side, m, h: yland_u.at[side, m, rem4(z + h)],
+        ),
+    )
     upper = ff // 2
 
     def hop_of(k):
@@ -375,23 +454,19 @@
             for g in range(4):
                 grad[g, upper:, lanes(yi)] = value[:, g * cols : (g + 1) * cols]
 
+            if extra:
+                extra(k)
             for turn, step in ((0, "far"), (1, "to_right"), (2, "to_left")):
 
                 @pl.when(k == turn)
                 def _(step=step):
                     each(first, step)
 
-            extra(k)
             return carry
 
         lax.fori_loop(0, 4, body, 0)
 
-    def while_down(k):
-        @pl.when(k == 2)
-        def _():
-            token_near("n")
-
-    weight_grad(ht, og, gd, gd1, while_down)
+    weight_grad(ht, og, gd, gd1, None)
 
     each(wu2, "near")
     each(wu2, "far")
@@ -400,13 +475,13 @@
         return part.at[block]
 
     xs = Scatter(
-        w, "x", x, x_right, x_left,
+        w, "x", "x", x, x_right, x_left,
         lambda i, p: part.at[i * 2 + c, pl.ds(p * half, half), :],
         lambda side, m: xland.at[side, m],
     )
-    cross_base = w.number(("cross", 0))
-    for k in range(1, 4):
-        w.number(("cross", k))
+    cross_base = [w.key(("c", k)) for k in range(4)][0]
+    cross_group = w.group("c")
+    w.bytes["c"] = size_of(cross)
 
     def product(index):
         at = pl.ds(pl.multiple_of(index * rows, rows), rows)
@@ -415,14 +490,14 @@
 
     def add_cross(k):
         index = rem4(x + hop_of(k)) * 2 + c
-        w.copy(cross_base + k, cross.at[k], cross.at[k], partner).wait_recv()
+        w.copy(cross_group, cross_base + k, cross.at[k], cross.at[k], partner).wait_recv()
         total = part[index].astype(F32) + cross[k].astype(F32)
         part[index] = total.astype(BF16)
 
     def input_grad(k, carry):
         xi = rem4(x + hop_of(k))
         product(xi * 2 + 1 - c)
-        w.copy(cross_base + k, part.at[xi * 2 + 1 - c], cross.at[k], partner).start()
+        w.copy(cross_group, cross_base + k, part.at[xi * 2 + 1 - c], cross.at[k], partner).start()
 
         @pl.when(k > 0)
         def _():
@@ -436,13 +511,17 @@
 
         product(xi * 2 + c)
 
+        @pl.when(k == 0)
+        def _():
+            token_near("n")
+
         @pl.when(k == 1)
         def _():
+            each(gd1, "middle")
+
+        @pl.when(k == 2)
+        def _():
             token_far("n")
-
-        @pl.when(k == 2)
-        def _():
-            each(gd1, "middle")
 
         return carry
 
@@ -451,20 +530,21 @@
     handed("n")
 
     def while_up(k):
-        @pl.when(k == 2)
-        def _():
-            xs.middle()
-
-        @pl.when(k == 3)
+        @pl.when(k == 1)
         def _():
             each(gd1, "finish")
             each(gd2, "far")
             each(gd2, "to_right")
             each(gd2, "to_left")
 
+        @pl.when(k == 2)
+        def _():
+            xs.middle()
+
     weight_grad(pgt, ni, gu, gu1, while_up)
 
-    each(gu1, "middle")
+    each(gu1, "add_first")
+    give(gu1, 2, 1, 3)
     each(gd2, "middle")
 
     def own_rows(out):
@@ -473,30 +553,59 @@
             lambda p: out.at[wd_rows(2 + p), :],
         )
 
-    for ring, out in zip(gd2, own_rows(dg)):
-        ring.finish(out)
-    down_out = pltpu.make_async_copy(dg, dg_hbm, local_sem.at[5])
-    down_out.start()
+    def settle(h):
+        for ring in gu1:
+            ring.settle(h)
+
+    each(gu1, "settle_near")
+    settle(2)
+    each(gu2, "far")
+    give(gu1, 0)
+    settle(1)
+    each(gu2, "to_right")
+    settle(3)
+    each(gu2, "to_left")
     w.drain("o")
     ig = og.at[pl.ds(0, rows), :]
     xs.finish(lambda p: og.at[pl.ds(p * half, half), :])
     input_out = pltpu.make_async_copy(ig, ig_hbm, local_sem.at[6])
     input_out.start()
-    each(gu1, "finish")
-    each(gu2, "far")
-    each(gu2, "to_right")
-    each(gu2, "to_left")
+    for ring, out in zip(gd2, own_rows(dg)):
+        ring.finish(out)
+    down_out = pltpu.make_async_copy(dg, dg_hbm, local_sem.at[5])
+    down_out.start()
     each(gu2, "middle")
+    settle(0)
     for ring, out in zip(gu2, own_rows(ug)):
         ring.finish(out)
     up_out = pltpu.make_async_copy(ug, ug_hbm, local_sem.at[7])
     up_out.start()
-    for k in range(4):
-        w.copy(cross_base + k, cross.at[k], cross.at[k], partner).wait_send()
-    w.drain()
+    for group in ("d", "u", "n", "D", "U", "x", "c"):
+        w.drain(group)
     down_out.wait()
     input_out.wait()
     up_out.wait()
+
+
+def deliver(ig_in, ug_in, dg_in, ig_out, ug_out, dg_out, ig, ug, dg, turned, sem):
+    into = [
+        pltpu.make_async_copy(src, dst, sem.at[i])
+        for i, (src, dst) in enumerate(((ug_in, ug), (ig_in, ig), (dg_in, dg)))
+    ]
+    for copy in into:
+        copy.start()
+    out = [
+        pltpu.make_async_copy(src, dst, sem.at[3 + i])
+        for i, (src, dst) in enumerate(((turned, ug_out), (ig, ig_out), (dg, dg_out)))
+    ]
+    into[0].wait()
+    turned[...] = ug[...].T
+    out[0].start()
+    for i in (1, 2):
+        into[i].wait()
+        out[i].start()
+    for copy in out:
+        copy.wait()
 
 
 def local(normed_input, pre_act, out_grad, up_weight, down_weight):
@@ -537,8 +646,8 @@
             *grads,
             pltpu.VMEM((ff, cols), F32),
             pltpu.VMEM((ff, cols), F32),
-            pltpu.SemaphoreType.DMA((SEMS,)),
-            pltpu.SemaphoreType.DMA((SEMS,)),
+            pltpu.SemaphoreType.DMA((SENDS,)),
+            pltpu.SemaphoreType.DMA((RECVS,)),
             pltpu.SemaphoreType.DMA((8,)),
         ],
         compiler_params=pltpu.CompilerParams(
@@ -548,7 +657,25 @@
         ),
         name="ffn_backward",
     )(normed_input, pre_act, out_grad, up_weight, down_weight)
-    return input_grad, up_grad.T, down_grad
+    return pl.pallas_call(
+        deliver,
+        out_shape=(
+            jax.ShapeDtypeStruct((rows, d), BF16),
+            jax.ShapeDtypeStruct((cols, ff), F32),
+            jax.ShapeDtypeStruct((ff, cols), F32),
+        ),
+        in_specs=[pl.BlockSpec(memory_space=pl.ANY)] * 3,
+        out_specs=(pl.BlockSpec(memory_space=pl.ANY),) * 3,
+        scratch_shapes=[
+            pltpu.VMEM((rows, d), BF16),
+            pltpu.VMEM((ff, cols), F32),
+            pltpu.VMEM((ff, cols), F32),
+            pltpu.VMEM((cols, ff), F32),
+            pltpu.SemaphoreType.DMA((6,)),
+        ],
+        compiler_params=pltpu.CompilerParams(vmem_limit_bytes=67043328),
+        name="deliver",
+    )(input_grad, up_grad, down_grad)
 
 
 def solution(mesh):

time: 114 us -> 101 us (0.89)
  Pallas kernels: 107 us -> 100 us
  local copies, waits for them, and re-layouts: 5.99 us -> 0 us
    pallas_call x1, Pallas kernels: 107 us -> 97.8 us  [local(): pl.pallas_call(kernel, out_shape=(jax.ShapeDtypeStruct((rows, d), BF16),...]
    unnamed x3 -> x0, local copies, waits for them, and re-layouts: 5.99 us -> none
    pallas_call x0 -> x1, Pallas kernels: none -> 2.52 us  [local(): pl.pallas_call(deliver, out_shape=(jax.ShapeDtypeStruct((rows, d), BF16),...]
where the time goes in v2:
time: 101 us
  Pallas kernels  100 us (99%)
    pallas_call x1, Pallas kernels, local(): pl.pallas_call(kernel, out_shape=(jax.ShapeDtypeStruct((rows, d), BF16),...  97.8 us
    pallas_call x1, Pallas kernels, local(): pl.pallas_call(deliver, out_shape=(jax.ShapeDtypeStruct((rows, d), BF16),...  2.52 us

profile of v2, /device:TPU:0, one launch (start us, length us, event | category | flops | bytes accessed | tf_op | source)
XLA Modules:
  0.0 101.0 jit_solution(14899112072283154884)
XLA Ops:
  0.6 97.8 %ffn_backward.1 = (bf16[192,2048]{1,0:T(8,128)(2,1)}, f32[1024,128]{1,0:T(8,128)}, f32[1024,128]{1,0:T(8,128)}) custom-call(bf16[192,2048]{1,0:T(8,128)(2,1)} %ni_hbm.1, bf16[1536,1024]{1,0:T(8,128)(2,1)} %pa_hbm.1, bf16[192,2048]{1,0:T(8,128)(2,1)} %og_hbm.1, bf16[128,1024]{1,0:T(8,128)(2,1)} %uw_hbm.1, bf16[1024,128]{1,0:T(8,128)(2,1)} %dw_hbm.1), custom_call_target="tpu_custom_call" | custom-call | tf_op jit(solution)/shard_map/ffn_backward/pallas_call | solution.py:623
  98.5 2.5 %deliver.1 = (bf16[192,2048]{1,0:T(8,128)(2,1)}, f32[128,1024]{1,0:T(8,128)}, f32[1024,128]{1,0:T(8,128)}) custom-call(bf16[192,2048]{1,0:T(8,128)(2,1)} %get-tuple-element.6.ig_in, f32[1024,128]{1,0:T(8,128)} %get-tuple-element.7.ug_in, f32[1024,128]{1,0:T(8,128)} %get-tuple-element.8.dg_in), custom_call_target="tpu_custom_call" | custom-call | tf_op jit(solution)/shard_map/deliver/pallas_call | solution.py:660

commit v3 on v2

--- a/solution.py
+++ b/solution.py
@@ -148,14 +148,16 @@
         self.put("last", 0, 2, 1, 0)
         self.put("last", 1, 2, 3, 1)
 
-    def finish(self, out=None):
+    def finish(self, store=None):
         self.w.recv((self.tag, "last"), 4 * self.size)
         for p, near, far in ((1, 0, 1), (0, 1, 0)):
             first, second = self.landing(near, 1), self.landing(far, 2)
             mine = self.at(0, p)
             total = mine[...].astype(F32) + first[...].astype(F32) + second[...].astype(F32)
-            target = mine if out is None else out(p)
-            target[...] = total.astype(target.dtype)
+            if store is None:
+                mine[...] = total.astype(BF16)
+            else:
+                store(p, total)
 
 
 class QuarterScatter(Scatter):
@@ -188,11 +190,11 @@
 
 def kernel(
     ni_hbm, pa_hbm, og_hbm, uw_hbm, dw_hbm,
-    ig_hbm, ug_hbm, dg_hbm,
-    ni, og, wd, wu, pg, ht, pgt, part, gd, gu,
+    ig, ug, dg,
+    ni, og, wd, wu, pg, ht, pgt, part, gd,
     cross, xland, zland_d, yland_d, yone_d, zone_d,
     zland_u, yland_u, yone_u, zone_u,
-    dg, ug, send_sem, recv_sem, local_sem,
+    send_sem, recv_sem, local_sem,
 ):
     fs, tp = lax.axis_index("fs"), lax.axis_index("tp")
     z, y, x, c = fs // 4, rem4(fs), tp // 2, lax.rem(tp, 2)
@@ -232,12 +234,11 @@
         pltpu.make_async_copy(src, dst, local_sem.at[i])
         for i, (src, dst) in enumerate(mine)
     ]
-    for copy in local:
-        copy.start()
-
     barrier = pltpu.get_barrier_semaphore()
     for device in (x_right, x_left, y_right, y_left, z_right, z_left, partner):
         pl.semaphore_signal(barrier, inc=1, device_id=device, device_id_type=MESH)
+    for copy in local:
+        copy.start()
     pl.semaphore_wait(barrier, 7)
 
     def wd_rows(p):
@@ -371,12 +372,14 @@
 
     def pre_grad(i, carry):
         at = pl.ds(pl.multiple_of(i * block, block), block)
-        weight = jnp.concatenate([wd[k] for k in range(4)], axis=1)
-        grad = nt(og[at, :], weight)
-        active = jnp.maximum(pg[at, :].astype(F32), 0.0)
-        value = (2.0 * active * grad).astype(BF16)
-        pg[at, :] = value
-        pgt[:, at] = value.T
+        for n in range(2):
+            units = pl.ds(n * ff // 2, ff // 2)
+            weight = jnp.concatenate([wd[k, units, :] for k in range(4)], axis=1)
+            grad = nt(og[at, :], weight)
+            active = jnp.maximum(pg[at, units].astype(F32), 0.0)
+            value = (2.0 * active * grad).astype(BF16)
+            pg[at, units] = value
+            pgt[units, at] = value.T
 
         @pl.when(i == 3)
         def _():
@@ -419,6 +422,7 @@
         )
 
     gd1, gd2 = grad_rings("D", gd, zland_d, yland_d, yone_d, zone_d)
+    gu = wd
     _, gu2 = grad_rings("U", gu, zland_u, yland_u, yone_u, zone_u)
     gu1 = (
         QuarterScatter(
@@ -483,10 +487,17 @@
     cross_group = w.group("c")
     w.bytes["c"] = size_of(cross)
 
-    def product(index):
-        at = pl.ds(pl.multiple_of(index * rows, rows), rows)
-        weight = wu[...].reshape(16 * urows, ff)
-        part[index] = nt(pg[at, :], weight).astype(BF16)
+    def product(xi):
+        at = pl.ds(pl.multiple_of(xi * 2 * rows, 2 * rows), 2 * rows)
+        for g in range(4):
+            value = nt(pg[at, :], wu[g].reshape(4 * urows, ff)).astype(BF16)
+            out = pl.ds(g * 4 * urows, 4 * urows)
+            part[xi * 2, :, out] = value[:rows]
+            part[xi * 2 + 1, :, out] = value[rows:]
+
+    def send_cross(k):
+        block = part.at[rem4(x + hop_of(k)) * 2 + 1 - c]
+        w.copy(cross_group, cross_base + k, block, cross.at[k], partner).start()
 
     def add_cross(k):
         index = rem4(x + hop_of(k)) * 2 + c
@@ -496,21 +507,19 @@
 
     def input_grad(k, carry):
         xi = rem4(x + hop_of(k))
-        product(xi * 2 + 1 - c)
-        w.copy(cross_group, cross_base + k, part.at[xi * 2 + 1 - c], cross.at[k], partner).start()
+        product(xi)
+        send_cross(k)
 
         @pl.when(k > 0)
         def _():
             add_cross(k - 1)
 
-        for turn, step in ((1, xs.far), (2, xs.to_right), (3, xs.to_left)):
+        for turn, step in ((1, xs.far), (2, xs.to_right)):
 
             @pl.when(k == turn)
             def _(step=step):
                 step()
 
-        product(xi * 2 + c)
-
         @pl.when(k == 0)
         def _():
             token_near("n")
@@ -525,9 +534,11 @@
 
         return carry
 
-    lax.fori_loop(0, 4, input_grad, 0)
-    add_cross(3)
+    lax.fori_loop(0, 3, input_grad, 0)
+    add_cross(2)
+    xs.to_left()
     handed("n")
+    w.drain("d")
 
     def while_up(k):
         @pl.when(k == 1)
@@ -543,15 +554,12 @@
 
     weight_grad(pgt, ni, gu, gu1, while_up)
 
+    product(x)
+    send_cross(3)
     each(gu1, "add_first")
     give(gu1, 2, 1, 3)
     each(gd2, "middle")
-
-    def own_rows(out):
-        return (
-            lambda p: out.at[wd_rows(p), :],
-            lambda p: out.at[wd_rows(2 + p), :],
-        )
+    add_cross(3)
 
     def settle(h):
         for ring in gu1:
@@ -565,46 +573,35 @@
     each(gu2, "to_right")
     settle(3)
     each(gu2, "to_left")
-    w.drain("o")
-    ig = og.at[pl.ds(0, rows), :]
-    xs.finish(lambda p: og.at[pl.ds(p * half, half), :])
-    input_out = pltpu.make_async_copy(ig, ig_hbm, local_sem.at[6])
-    input_out.start()
-    for ring, out in zip(gd2, own_rows(dg)):
-        ring.finish(out)
-    down_out = pltpu.make_async_copy(dg, dg_hbm, local_sem.at[5])
-    down_out.start()
+
+    def store_rows(p, total):
+        ig[pl.ds(p * half, half), :] = total.astype(BF16)
+
+    xs.finish(store_rows)
+    for i, ring in enumerate(gd2):
+
+        def store_down(p, total, i=i):
+            dg[wd_rows(2 * i + p), :] = total
+
+        ring.finish(store_down)
     each(gu2, "middle")
     settle(0)
-    for ring, out in zip(gu2, own_rows(ug)):
-        ring.finish(out)
-    up_out = pltpu.make_async_copy(ug, ug_hbm, local_sem.at[7])
-    up_out.start()
-    for group in ("d", "u", "n", "D", "U", "x", "c"):
+    for i, ring in enumerate(gu2):
+
+        def store_up(p, total, i=i):
+            ug[:, wd_rows(2 * i + p)] = total.T
+
+        ring.finish(store_up)
+    for group in ("u", "o", "n", "D", "U", "x", "c"):
         w.drain(group)
-    down_out.wait()
-    input_out.wait()
-    up_out.wait()
-
-
-def deliver(ig_in, ug_in, dg_in, ig_out, ug_out, dg_out, ig, ug, dg, turned, sem):
-    into = [
-        pltpu.make_async_copy(src, dst, sem.at[i])
-        for i, (src, dst) in enumerate(((ug_in, ug), (ig_in, ig), (dg_in, dg)))
-    ]
-    for copy in into:
+
+
+def deliver(*refs):
+    sem = refs[-1]
+    copies = [pltpu.make_async_copy(refs[i], refs[3 + i], sem.at[i]) for i in range(3)]
+    for copy in copies:
         copy.start()
-    out = [
-        pltpu.make_async_copy(src, dst, sem.at[3 + i])
-        for i, (src, dst) in enumerate(((turned, ug_out), (ig, ig_out), (dg, dg_out)))
-    ]
-    into[0].wait()
-    turned[...] = ug[...].T
-    out[0].start()
-    for i in (1, 2):
-        into[i].wait()
-        out[i].start()
-    for copy in out:
+    for copy in copies:
         copy.wait()
 
 
@@ -623,12 +620,12 @@
     input_grad, up_grad, down_grad = pl.pallas_call(
         kernel,
         out_shape=(
-            jax.ShapeDtypeStruct((rows, d), BF16),
-            jax.ShapeDtypeStruct((ff, cols), F32),
-            jax.ShapeDtypeStruct((ff, cols), F32),
+            pltpu.VMEM((rows, d), BF16),
+            pltpu.VMEM((cols, ff), F32),
+            pltpu.VMEM((ff, cols), F32),
         ),
-        in_specs=[pl.BlockSpec(memory_space=pl.ANY)] * 5,
-        out_specs=(pl.BlockSpec(memory_space=pl.ANY),) * 3,
+        in_specs=[pl.BlockSpec(memory_space=pltpu.HBM)] * 5,
+        out_specs=(pl.BlockSpec(memory_space=pltpu.VMEM),) * 3,
         scratch_shapes=[
             pltpu.VMEM((tokens, d), BF16),
             pltpu.VMEM((tokens, d), BF16),
@@ -639,21 +636,18 @@
             pltpu.VMEM((ff, tokens), BF16),
             pltpu.VMEM((8, rows, d), BF16),
             pltpu.VMEM((4, ff, 4 * cols), BF16),
-            pltpu.VMEM((4, ff, 4 * cols), BF16),
             pltpu.VMEM((4, rows, d), BF16),
             pltpu.VMEM((2, 3, half, d), BF16),
             *grads,
             *grads,
-            pltpu.VMEM((ff, cols), F32),
-            pltpu.VMEM((ff, cols), F32),
             pltpu.SemaphoreType.DMA((SENDS,)),
             pltpu.SemaphoreType.DMA((RECVS,)),
-            pltpu.SemaphoreType.DMA((8,)),
+            pltpu.SemaphoreType.DMA((5,)),
         ],
         compiler_params=pltpu.CompilerParams(
             collective_id=0,
             has_side_effects=True,
-            vmem_limit_bytes=67043328,
+            vmem_limit_bytes=62800000,
         ),
         name="ffn_backward",
     )(normed_input, pre_act, out_grad, up_weight, down_weight)
@@ -666,14 +660,8 @@
         ),
         in_specs=[pl.BlockSpec(memory_space=pl.ANY)] * 3,
         out_specs=(pl.BlockSpec(memory_space=pl.ANY),) * 3,
-        scratch_shapes=[
-            pltpu.VMEM((rows, d), BF16),
-            pltpu.VMEM((ff, cols), F32),
-            pltpu.VMEM((ff, cols), F32),
-            pltpu.VMEM((cols, ff), F32),
-            pltpu.SemaphoreType.DMA((6,)),
-        ],
-        compiler_params=pltpu.CompilerParams(vmem_limit_bytes=67043328),
+        scratch_shapes=[pltpu.SemaphoreType.DMA((3,))],
+        compiler_params=pltpu.CompilerParams(vmem_limit_bytes=4 * 2**20),
         name="deliver",
     )(input_grad, up_grad, down_grad)
 

time: 101 us -> 96 us (0.950)
  Pallas kernels: 100 us -> 95.1 us
    pallas_call x1, Pallas kernels: 97.8 us -> 93.8 us  [local(): pl.pallas_call(kernel, out_shape=(pltpu.VMEM((rows, d), BF16), pltpu.VMEM...]
    pallas_call x1, Pallas kernels: 2.52 us -> 1.25 us  [local(): pl.pallas_call(deliver, out_shape=(jax.ShapeDtypeStruct((rows, d), BF16),...]
where the time goes in v3:
time: 96 us; the launch traced here: 95.7 us
  Pallas kernels  95.1 us (99%)
    pallas_call x1, Pallas kernels, local(): pl.pallas_call(kernel, out_shape=(pltpu.VMEM((rows, d), BF16), pltpu.VMEM...  93.8 us

profile of v3, /device:TPU:0, one launch (start us, length us, event | category | flops | bytes accessed | tf_op | source)
XLA Modules:
  0.0 95.7 jit_solution(6762405897882397622)
XLA Ops:
  0.6 93.8 %ffn_backward.1 = (bf16[192,2048]{1,0:T(8,128)(2,1)S(1)}, f32[128,1024]{1,0:T(8,128)S(1)}, f32[1024,128]{1,0:T(8,128)S(1)}) custom-call(bf16[192,2048]{1,0:T(8,128)(2,1)} %ni_hbm.1, bf16[1536,1024]{1,0:T(8,128)(2,1)} %pa_hbm.1, bf16[192,2048]{1,0:T(8,128)(2,1)} %og_hbm.1, bf16[128,1024]{1,0:T(8,128)(2,1)} %uw_hbm.1, bf16[1024,128]{1,0:T(8,128)(2,1)} %dw_hbm.1), custom_call_target="tpu_custom_call" | custom-call | tf_op jit(solution)/shard_map/ffn_backward/pallas_call | solution.py:620
  94.4 1.3 %deliver.1 = (bf16[192,2048]{1,0:T(8,128)(2,1)}, f32[128,1024]{1,0:T(8,128)}, f32[1024,128]{1,0:T(8,128)}) custom-call(bf16[192,2048]{1,0:T(8,128)(2,1)S(1)} %get-tuple-element.6.refs_0_, f32[128,1024]{1,0:T(8,128)S(1)} %get-tuple-element.7.refs_1_, f32[1024,128]{1,0:T(8,128)S(1)} %get-tuple-element.8.refs_2_), custom_call_target="tpu_custom_call" | custom-call | tf_op jit(solution)/shard_map/deliver/pallas_call | solution.py:654

commit v4 on v3

--- a/solution.py
+++ b/solution.py
@@ -10,7 +10,7 @@
 MESH = pl.DeviceIdType.MESH
 F32 = jnp.float32
 BF16 = jnp.bfloat16
-SENDS, RECVS = 8, 64
+SENDS, RECVS = 8, 38
 
 
 def rem4(value):
@@ -65,10 +65,16 @@
 
 
 class Gather:
+    share = 1
+
     def __init__(self, wires, group, tag, pos, right, left, piece):
         self.w, self.group, self.tag, self.pos = wires, group, tag, pos
         self.right, self.left, self.piece = right, left, piece
         self.size = size_of(piece(pos, 0))
+
+    def wait(self, name, pieces):
+        if self.share:
+            self.w.recv((self.tag, name), self.share * pieces * self.size)
 
     def at(self, hop, p):
         return self.piece(rem4(self.pos + hop), p)
@@ -84,15 +90,15 @@
         self.put("near", 0, 0, self.left)
 
     def forward(self):
-        self.w.recv((self.tag, "first"), 2 * self.size)
+        self.wait("first", 2)
         self.put("far", 3, 0, self.right)
         self.put("far", 1, 1, self.left)
 
     def near(self):
-        self.w.recv((self.tag, "near"), 2 * self.size)
+        self.wait("near", 2)
 
     def far(self):
-        self.w.recv((self.tag, "far"), 2 * self.size)
+        self.wait("far", 2)
 
 
 class QuarterGather(Gather):
@@ -109,11 +115,17 @@
 
 
 class Scatter:
+    share = 1
+
     def __init__(self, wires, group, tag, pos, right, left, piece, landing):
         self.w, self.group, self.tag, self.pos = wires, group, tag, pos
         self.right, self.left = right, left
         self.piece, self.landing = piece, landing
         self.size = size_of(piece(pos, 0))
+
+    def wait(self, name, quarters):
+        if self.share:
+            self.w.recv((self.tag, name), self.share * quarters * self.size // 4)
 
     def at(self, hop, p):
         return self.piece(rem4(self.pos + hop), p)
@@ -138,7 +150,7 @@
         self.put("last", 1, 1, 3, 0)
 
     def add_first(self):
-        self.w.recv((self.tag, "first"), 2 * self.size)
+        self.wait("first", 8)
         for side, hop, p in ((0, 1, 0), (1, 3, 1)):
             came, mine = self.landing(side, 0), self.at(hop, p)
             mine[...] = (mine[...].astype(F32) + came[...].astype(F32)).astype(BF16)
@@ -149,7 +161,7 @@
         self.put("last", 1, 2, 3, 1)
 
     def finish(self, store=None):
-        self.w.recv((self.tag, "last"), 4 * self.size)
+        self.wait("last", 16)
         for p, near, far in ((1, 0, 1), (0, 1, 0)):
             first, second = self.landing(near, 1), self.landing(far, 2)
             mine = self.at(0, p)
@@ -177,15 +189,20 @@
                 )
 
     def settle_near(self):
-        self.w.recv((self.tag, "last"), 2 * self.size)
+        self.wait("last", 8)
 
     def settle(self, h):
-        self.w.recv((self.tag, h), self.size // 2)
+        self.wait(h, 2)
         for p, near, far in ((1, 0, 1), (0, 1, 0)):
             first, second = self.landed(near, 1, h), self.landed(far, 2, h)
             mine = self.quarter(self.pos, p, h)
             total = mine[...].astype(F32) + first[...].astype(F32) + second[...].astype(F32)
             mine[...] = total.astype(BF16)
+
+
+def paired(first, second):
+    second.tag, first.share, second.share = first.tag, 2, 0
+    return first, second
 
 
 def kernel(
@@ -283,6 +300,9 @@
         lambda zi, p: wu.at[zi, :, wu_rows(p), :],
         lambda yi, p: wu.at[:, yi, wu_rows(p), :],
     )
+
+    for pair in (wd1, wd2, wu1, wu2):
+        paired(*pair)
 
     def token_piece(ref, core):
         def piece(i, p):
@@ -363,9 +383,9 @@
     each(wd2, "forward")
     each(wu2, "own")
     token_near("o")
+    token_far("o")
     each(wd2, "near")
     each(wd2, "far")
-    token_far("o")
     handed("o")
 
     block = 256
@@ -440,6 +460,8 @@
             lambda side, m, h: yland_u.at[side, m, rem4(z + h)],
         ),
     )
+    for pair in (gd1, gd2, gu1, gu2):
+        paired(*pair)
     upper = ff // 2
 
     def hop_of(k):
@@ -510,16 +532,6 @@
         product(xi)
         send_cross(k)
 
-        @pl.when(k > 0)
-        def _():
-            add_cross(k - 1)
-
-        for turn, step in ((1, xs.far), (2, xs.to_right)):
-
-            @pl.when(k == turn)
-            def _(step=step):
-                step()
-
         @pl.when(k == 0)
         def _():
             token_near("n")
@@ -527,20 +539,27 @@
         @pl.when(k == 1)
         def _():
             each(gd1, "middle")
+            add_cross(0)
+            xs.far()
 
         @pl.when(k == 2)
         def _():
             token_far("n")
+            add_cross(1)
+            xs.to_right()
 
         return carry
 
     lax.fori_loop(0, 3, input_grad, 0)
-    add_cross(2)
-    xs.to_left()
     handed("n")
     w.drain("d")
 
     def while_up(k):
+        @pl.when(k == 0)
+        def _():
+            add_cross(2)
+            xs.to_left()
+
         @pl.when(k == 1)
         def _():
             each(gd1, "finish")
@@ -574,6 +593,9 @@
     settle(3)
     each(gu2, "to_left")
 
+    each(gu2, "middle")
+    settle(0)
+
     def store_rows(p, total):
         ig[pl.ds(p * half, half), :] = total.astype(BF16)
 
@@ -584,8 +606,6 @@
             dg[wd_rows(2 * i + p), :] = total
 
         ring.finish(store_down)
-    each(gu2, "middle")
-    settle(0)
     for i, ring in enumerate(gu2):
 
         def store_up(p, total, i=i):

time: 96 us -> 95.6 us (level)
  no operation moved by 1% of the time
where the time goes in v4:
time: 95.6 us; the launch traced here: 95.5 us
  Pallas kernels  94.9 us (99%)
    pallas_call x1, Pallas kernels, local(): pl.pallas_call(kernel, out_shape=(pltpu.VMEM((rows, d), BF16), pltpu.VMEM...  93.6 us

profile of v4, /device:TPU:0, one launch (start us, length us, event | category | flops | bytes accessed | tf_op | source)
XLA Modules:
  0.0 95.5 jit_solution(15856662380422632377)
XLA Ops:
  0.6 93.6 %ffn_backward.1 = (bf16[192,2048]{1,0:T(8,128)(2,1)S(1)}, f32[128,1024]{1,0:T(8,128)S(1)}, f32[1024,128]{1,0:T(8,128)S(1)}) custom-call(bf16[192,2048]{1,0:T(8,128)(2,1)} %ni_hbm.1, bf16[1536,1024]{1,0:T(8,128)(2,1)} %pa_hbm.1, bf16[192,2048]{1,0:T(8,128)(2,1)} %og_hbm.1, bf16[128,1024]{1,0:T(8,128)(2,1)} %uw_hbm.1, bf16[1024,128]{1,0:T(8,128)(2,1)} %dw_hbm.1), custom_call_target="tpu_custom_call" | custom-call | tf_op jit(solution)/shard_map/ffn_backward/pallas_call | solution.py:640
  94.3 1.3 %deliver.1 = (bf16[192,2048]{1,0:T(8,128)(2,1)}, f32[128,1024]{1,0:T(8,128)}, f32[1024,128]{1,0:T(8,128)}) custom-call(bf16[192,2048]{1,0:T(8,128)(2,1)S(1)} %get-tuple-element.6.refs_0_, f32[128,1024]{1,0:T(8,128)S(1)} %get-tuple-element.7.refs_1_, f32[1024,128]{1,0:T(8,128)S(1)} %get-tuple-element.8.refs_2_), custom_call_target="tpu_custom_call" | custom-call | tf_op jit(solution)/shard_map/deliver/pallas_call | solution.py:674

commit v5 on v4

--- a/solution.py
+++ b/solution.py
@@ -188,11 +188,19 @@
                     self.right if side == 0 else self.left,
                 )
 
-    def settle_near(self):
-        self.wait("last", 8)
+    def near(self, *members):
+        for h in members:
+            for side, hop, p in ((0, 1, 1), (1, 3, 0)):
+                self.w.send(
+                    self.group,
+                    (self.tag, h),
+                    self.quarter(rem4(self.pos + hop), p, h),
+                    self.landed(side, 1, h),
+                    self.right if side == 0 else self.left,
+                )
 
     def settle(self, h):
-        self.wait(h, 2)
+        self.wait(h, 4)
         for p, near, far in ((1, 0, 1), (0, 1, 0)):
             first, second = self.landed(near, 1, h), self.landed(far, 2, h)
             mine = self.quarter(self.pos, p, h)
@@ -401,7 +409,7 @@
             pg[at, units] = value
             pgt[units, at] = value.T
 
-        @pl.when(i == 3)
+        @pl.when(i == 2)
         def _():
             each(wu2, "forward")
 
@@ -467,7 +475,7 @@
     def hop_of(k):
         return jnp.where(k == 0, 2, jnp.where(k == 1, 1, jnp.where(k == 2, 3, 0)))
 
-    def weight_grad(left, right, grad, first, extra):
+    def weight_grad(left, right, grad, first, steps, extra):
         def body(k, carry):
             zi, yi = rem4(z + hop_of(k)), rem4(y + hop_of(k))
             strip = right[:, pl.ds(pl.multiple_of(zi * wide, wide), wide)]
@@ -482,7 +490,7 @@
 
             if extra:
                 extra(k)
-            for turn, step in ((0, "far"), (1, "to_right"), (2, "to_left")):
+            for turn, step in enumerate(steps):
 
                 @pl.when(k == turn)
                 def _(step=step):
@@ -492,7 +500,7 @@
 
         lax.fori_loop(0, 4, body, 0)
 
-    weight_grad(ht, og, gd, gd1, None)
+    weight_grad(ht, og, gd, gd1, ("far", "to_right", "to_left"), None)
 
     each(wu2, "near")
     each(wu2, "far")
@@ -530,6 +538,11 @@
     def input_grad(k, carry):
         xi = rem4(x + hop_of(k))
         product(xi)
+
+        @pl.when(k == 2)
+        def _():
+            token_far("n")
+
         send_cross(k)
 
         @pl.when(k == 0)
@@ -544,7 +557,6 @@
 
         @pl.when(k == 2)
         def _():
-            token_far("n")
             add_cross(1)
             xs.to_right()
 
@@ -553,6 +565,10 @@
     lax.fori_loop(0, 3, input_grad, 0)
     handed("n")
     w.drain("d")
+
+    def near(*members):
+        for ring in gu1:
+            ring.near(*members)
 
     def while_up(k):
         @pl.when(k == 0)
@@ -569,30 +585,32 @@
 
         @pl.when(k == 2)
         def _():
+            near(2)
             xs.middle()
 
-    weight_grad(pgt, ni, gu, gu1, while_up)
-
-    product(x)
-    send_cross(3)
-    each(gu1, "add_first")
-    give(gu1, 2, 1, 3)
-    each(gd2, "middle")
-    add_cross(3)
+    weight_grad(pgt, ni, gu, gu1, ("far",), while_up)
 
     def settle(h):
         for ring in gu1:
             ring.settle(h)
 
-    each(gu1, "settle_near")
+    near(1)
+    each(gu1, "add_first")
+    give(gu1, 2, 1)
+    near(3)
+    give(gu1, 3)
+    product(x)
+    send_cross(3)
+    each(gd2, "middle")
     settle(2)
     each(gu2, "far")
+    near(0)
     give(gu1, 0)
     settle(1)
     each(gu2, "to_right")
     settle(3)
     each(gu2, "to_left")
-
+    add_cross(3)
     each(gu2, "middle")
     settle(0)
 

time: 95.6 us -> 95.2 us (level)
  no operation moved by 1% of the time
where the time goes in v5:
time: 95.2 us; the launch traced here: 95 us
  Pallas kernels  94.4 us (99%)
    pallas_call x1, Pallas kernels, local(): pl.pallas_call(kernel, out_shape=(pltpu.VMEM((rows, d), BF16), pltpu.VMEM...  93.2 us

profile of v5, /device:TPU:0, one launch (start us, length us, event | category | flops | bytes accessed | tf_op | source)
XLA Modules:
  0.0 95.0 jit_solution(12430759911956549228)
XLA Ops:
  0.6 93.2 %ffn_backward.1 = (bf16[192,2048]{1,0:T(8,128)(2,1)S(1)}, f32[128,1024]{1,0:T(8,128)S(1)}, f32[1024,128]{1,0:T(8,128)S(1)}) custom-call(bf16[192,2048]{1,0:T(8,128)(2,1)} %ni_hbm.1, bf16[1536,1024]{1,0:T(8,128)(2,1)} %pa_hbm.1, bf16[192,2048]{1,0:T(8,128)(2,1)} %og_hbm.1, bf16[128,1024]{1,0:T(8,128)(2,1)} %uw_hbm.1, bf16[1024,128]{1,0:T(8,128)(2,1)} %dw_hbm.1), custom_call_target="tpu_custom_call" | custom-call | tf_op jit(solution)/shard_map/ffn_backward/pallas_call | solution.py:658
  93.8 1.3 %deliver.1 = (bf16[192,2048]{1,0:T(8,128)(2,1)}, f32[128,1024]{1,0:T(8,128)}, f32[1024,128]{1,0:T(8,128)}) custom-call(bf16[192,2048]{1,0:T(8,128)(2,1)S(1)} %get-tuple-element.6.refs_0_, f32[128,1024]{1,0:T(8,128)S(1)} %get-tuple-element.7.refs_1_, f32[1024,128]{1,0:T(8,128)S(1)} %get-tuple-element.8.refs_2_), custom_call_target="tpu_custom_call" | custom-call | tf_op jit(solution)/shard_map/deliver/pallas_call | solution.py:692

commit v6 on v5

--- a/solution.py
+++ b/solution.py
@@ -116,6 +116,7 @@
 
 class Scatter:
     share = 1
+    near_name = "last"
 
     def __init__(self, wires, group, tag, pos, right, left, piece, landing):
         self.w, self.group, self.tag, self.pos = wires, group, tag, pos
@@ -144,10 +145,10 @@
         self.put("first", 1, 0, 2, 1)
 
     def to_right(self):
-        self.put("last", 0, 1, 1, 1)
+        self.put(self.near_name, 0, 1, 1, 1)
 
     def to_left(self):
-        self.put("last", 1, 1, 3, 0)
+        self.put(self.near_name, 1, 1, 3, 0)
 
     def add_first(self):
         self.wait("first", 8)
@@ -170,6 +171,20 @@
                 mine[...] = total.astype(BF16)
             else:
                 store(p, total)
+
+
+class StagedScatter(Scatter):
+    near_name = "near"
+
+    def begin(self, store):
+        self.wait("near", 8)
+        for p, side in ((1, 0), (0, 1)):
+            store(p, self.at(0, p)[...].astype(F32) + self.landing(side, 1)[...].astype(F32))
+
+    def end(self, add):
+        self.wait("last", 8)
+        for p, side in ((1, 1), (0, 0)):
+            add(p, self.landing(side, 2)[...])
 
 
 class QuarterScatter(Scatter):
@@ -421,7 +436,7 @@
 
     lax.fori_loop(0, tokens // block, pre_grad, 0)
 
-    def grad_rings(tag, grad, zland, yland, yone, zone):
+    def grad_rings(tag, grad, zland, yland, yone, zone, kind):
         return (
             (
                 Scatter(
@@ -436,12 +451,12 @@
                 ),
             ),
             (
-                Scatter(
+                kind(
                     w, tag, tag + "a2", y, y_right, y_left,
                     lambda i, p: grad.at[z, wd_rows(p), lanes(i)],
                     lambda side, m: yone.at[side, m],
                 ),
-                Scatter(
+                kind(
                     w, tag, tag + "b2", z, z_right, z_left,
                     lambda i, p: grad.at[i, wd_rows(2 + p), lanes(y)],
                     lambda side, m: zone.at[side, m],
@@ -449,9 +464,9 @@
             ),
         )
 
-    gd1, gd2 = grad_rings("D", gd, zland_d, yland_d, yone_d, zone_d)
+    gd1, gd2 = grad_rings("D", gd, zland_d, yland_d, yone_d, zone_d, Scatter)
     gu = wd
-    _, gu2 = grad_rings("U", gu, zland_u, yland_u, yone_u, zone_u)
+    _, gu2 = grad_rings("U", gu, zland_u, yland_u, yone_u, zone_u, StagedScatter)
     gu1 = (
         QuarterScatter(
             w, "U", "Ua1", z, z_right, z_left,
@@ -613,6 +628,12 @@
     add_cross(3)
     each(gu2, "middle")
     settle(0)
+    for i, ring in enumerate(gu2):
+
+        def store_up(p, total, i=i):
+            ug[:, wd_rows(2 * i + p)] = total.T
+
+        ring.begin(store_up)
 
     def store_rows(p, total):
         ig[pl.ds(p * half, half), :] = total.astype(BF16)
@@ -626,10 +647,11 @@
         ring.finish(store_down)
     for i, ring in enumerate(gu2):
 
-        def store_up(p, total, i=i):
-            ug[:, wd_rows(2 * i + p)] = total.T
-
-        ring.finish(store_up)
+        def add_up(p, came, i=i):
+            at = wd_rows(2 * i + p)
+            ug[:, at] = ug[:, at] + came.T.astype(F32)
+
+        ring.end(add_up)
     for group in ("u", "o", "n", "D", "U", "x", "c"):
         w.drain(group)
 

time: 95.2 us -> 95.1 us (level)
  no operation moved by 1% of the time
where the time goes in v6:
time: 95.1 us; the launch traced here: 95 us
  Pallas kernels  94.3 us (99%)
    pallas_call x1, Pallas kernels, local(): pl.pallas_call(kernel, out_shape=(pltpu.VMEM((rows, d), BF16), pltpu.VMEM...  93.1 us

profile of v6, /device:TPU:0, one launch (start us, length us, event | category | flops | bytes accessed | tf_op | source)
XLA Modules:
  0.0 95.0 jit_solution(3593013537889735432)
XLA Ops:
  0.6 93.1 %ffn_backward.1 = (bf16[192,2048]{1,0:T(8,128)(2,1)S(1)}, f32[128,1024]{1,0:T(8,128)S(1)}, f32[1024,128]{1,0:T(8,128)S(1)}) custom-call(bf16[192,2048]{1,0:T(8,128)(2,1)} %ni_hbm.1, bf16[1536,1024]{1,0:T(8,128)(2,1)} %pa_hbm.1, bf16[192,2048]{1,0:T(8,128)(2,1)} %og_hbm.1, bf16[128,1024]{1,0:T(8,128)(2,1)} %uw_hbm.1, bf16[1024,128]{1,0:T(8,128)(2,1)} %dw_hbm.1), custom_call_target="tpu_custom_call" | custom-call | tf_op jit(solution)/shard_map/ffn_backward/pallas_call | solution.py:680
  93.7 1.3 %deliver.1 = (bf16[192,2048]{1,0:T(8,128)(2,1)}, f32[128,1024]{1,0:T(8,128)}, f32[1024,128]{1,0:T(8,128)}) custom-call(bf16[192,2048]{1,0:T(8,128)(2,1)S(1)} %get-tuple-element.6.refs_0_, f32[128,1024]{1,0:T(8,128)S(1)} %get-tuple-element.7.refs_1_, f32[1024,128]{1,0:T(8,128)S(1)} %get-tuple-element.8.refs_2_), custom_call_target="tpu_custom_call" | custom-call | tf_op jit(solution)/shard_map/deliver/pallas_call | solution.py:714

commit v7 on v5

--- a/solution.py
+++ b/solution.py
@@ -476,10 +476,15 @@
         return jnp.where(k == 0, 2, jnp.where(k == 1, 1, jnp.where(k == 2, 3, 0)))
 
     def weight_grad(left, right, grad, first, steps, extra):
+        def launch(k, ring):
+            for turn, step in enumerate(steps):
+                pl.when(k == turn)(getattr(ring, step))
+
         def body(k, carry):
             zi, yi = rem4(z + hop_of(k)), rem4(y + hop_of(k))
             strip = right[:, pl.ds(pl.multiple_of(zi * wide, wide), wide)]
             grad[zi, :upper, :] = nn(left[:upper, :], strip).astype(BF16)
+            launch(k, first[0])
             strip = jnp.concatenate(
                 [right[:, pl.ds(pl.multiple_of(g * wide + yi * cols, cols), cols)] for g in range(4)],
                 axis=1,
@@ -487,14 +492,9 @@
             value = nn(left[upper:, :], strip).astype(BF16)
             for g in range(4):
                 grad[g, upper:, lanes(yi)] = value[:, g * cols : (g + 1) * cols]
-
+            launch(k, first[1])
             if extra:
                 extra(k)
-            for turn, step in enumerate(steps):
-
-                @pl.when(k == turn)
-                def _(step=step):
-                    each(first, step)
 
             return carry
 

time: 95.2 us -> 95.1 us (level)
  no operation moved by 1% of the time
where the time goes in v7:
time: 95.1 us; the launch traced here: 95 us
  Pallas kernels  94.4 us (99%)
    pallas_call x1, Pallas kernels, local(): pl.pallas_call(kernel, out_shape=(pltpu.VMEM((rows, d), BF16), pltpu.VMEM...  93.1 us

profile of v7, /device:TPU:0, one launch (start us, length us, event | category | flops | bytes accessed | tf_op | source)
XLA Modules:
  0.0 95.0 jit_solution(3133943453826379302)
XLA Ops:
  0.6 93.1 %ffn_backward.1 = (bf16[192,2048]{1,0:T(8,128)(2,1)S(1)}, f32[128,1024]{1,0:T(8,128)S(1)}, f32[1024,128]{1,0:T(8,128)S(1)}) custom-call(bf16[192,2048]{1,0:T(8,128)(2,1)} %ni_hbm.1, bf16[1536,1024]{1,0:T(8,128)(2,1)} %pa_hbm.1, bf16[192,2048]{1,0:T(8,128)(2,1)} %og_hbm.1, bf16[128,1024]{1,0:T(8,128)(2,1)} %uw_hbm.1, bf16[1024,128]{1,0:T(8,128)(2,1)} %dw_hbm.1), custom_call_target="tpu_custom_call" | custom-call | tf_op jit(solution)/shard_map/ffn_backward/pallas_call | solution.py:658
  93.7 1.3 %deliver.1 = (bf16[192,2048]{1,0:T(8,128)(2,1)}, f32[128,1024]{1,0:T(8,128)}, f32[1024,128]{1,0:T(8,128)}) custom-call(bf16[192,2048]{1,0:T(8,128)(2,1)S(1)} %get-tuple-element.6.refs_0_, f32[128,1024]{1,0:T(8,128)S(1)} %get-tuple-element.7.refs_1_, f32[1024,128]{1,0:T(8,128)S(1)} %get-tuple-element.8.refs_2_), custom_call_target="tpu_custom_call" | custom-call | tf_op jit(solution)/shard_map/deliver/pallas_call | solution.py:692

commit v8 on v5

--- a/solution.py
+++ b/solution.py
@@ -10,7 +10,7 @@
 MESH = pl.DeviceIdType.MESH
 F32 = jnp.float32
 BF16 = jnp.bfloat16
-SENDS, RECVS = 8, 38
+SENDS, RECVS = 8, 37
 
 
 def rem4(value):
@@ -262,8 +262,8 @@
     barrier = pltpu.get_barrier_semaphore()
     for device in (x_right, x_left, y_right, y_left, z_right, z_left, partner):
         pl.semaphore_signal(barrier, inc=1, device_id=device, device_id_type=MESH)
-    for copy in local:
-        copy.start()
+    for i in (0, 2, 1, 3, 4):
+        local[i].start()
     pl.semaphore_wait(barrier, 7)
 
     def wd_rows(p):
@@ -367,12 +367,12 @@
 
     local[0].wait()
     each(wd1, "own")
-    local[1].wait()
-    token_own("o")
     local[2].wait()
     each(wu1, "own")
     give(wd2, 0, 0)
     give(wd2, 1, 0)
+    local[1].wait()
+    token_own("o")
     local[3].wait()
     hidden(6, 0)
     each(wd1, "forward")

time: 95.2 us -> 95.1 us (level)
  no operation moved by 1% of the time
where the time goes in v8:
time: 95.1 us; the launch traced here: 95 us
  Pallas kernels  94.4 us (99%)
    pallas_call x1, Pallas kernels, local(): pl.pallas_call(kernel, out_shape=(pltpu.VMEM((rows, d), BF16), pltpu.VMEM...  93.1 us

profile of v8, /device:TPU:0, one launch (start us, length us, event | category | flops | bytes accessed | tf_op | source)
XLA Modules:
  0.0 95.0 jit_solution(15241693602553351977)
XLA Ops:
  0.6 93.1 %ffn_backward.1 = (bf16[192,2048]{1,0:T(8,128)(2,1)S(1)}, f32[128,1024]{1,0:T(8,128)S(1)}, f32[1024,128]{1,0:T(8,128)S(1)}) custom-call(bf16[192,2048]{1,0:T(8,128)(2,1)} %ni_hbm.1, bf16[1536,1024]{1,0:T(8,128)(2,1)} %pa_hbm.1, bf16[192,2048]{1,0:T(8,128)(2,1)} %og_hbm.1, bf16[128,1024]{1,0:T(8,128)(2,1)} %uw_hbm.1, bf16[1024,128]{1,0:T(8,128)(2,1)} %dw_hbm.1), custom_call_target="tpu_custom_call" | custom-call | tf_op jit(solution)/shard_map/ffn_backward/pallas_call | solution.py:658
  93.8 1.3 %deliver.1 = (bf16[192,2048]{1,0:T(8,128)(2,1)}, f32[128,1024]{1,0:T(8,128)}, f32[1024,128]{1,0:T(8,128)}) custom-call(bf16[192,2048]{1,0:T(8,128)(2,1)S(1)} %get-tuple-element.6.refs_0_, f32[128,1024]{1,0:T(8,128)S(1)} %get-tuple-element.7.refs_1_, f32[1024,128]{1,0:T(8,128)S(1)} %get-tuple-element.8.refs_2_), custom_call_target="tpu_custom_call" | custom-call | tf_op jit(solution)/shard_map/deliver/pallas_call | solution.py:692
